TPU v7x, 256 devices: a whole 4x4x8 slice. The times are simulated.
256 devices in a mesh: ep: 64 (over z, y, core), tp: 4 (over x).
Axes of the slice: x: 4, y: 4, z: 8, core: 2. Of those that a mesh axis runs over, the one named last changes fastest.
Arguments:
- glu_value: bfloat16 [32768, 1024], P('ep', 'tp'), may hold values from -6 to 6
- glu_gate: bfloat16 [32768, 1024], P('ep', 'tp'), may hold values from -12 to 12
- conv_kernel: float32 [31, 1024], P(None, 'tp'), may hold values from -11.49474 to 11.49474
- ln_gain: float32 [1024], P('tp'), may hold values from 0.1 to 1.9
- out_weight: bfloat16 [1024, 2048], P('tp'), may hold values from -0.1875 to 0.1875
- moe_input: bfloat16 [16384, 2048], P('ep'), may hold values from -6 to 6
- moe_gain: float32 [2048], replicated, may hold values from 0.1 to 1.9
- gate_weight: bfloat16 [64, 2048, 3072], P('ep', None, 'tp'), may hold values from -0.125 to 0.125
- up_weight: bfloat16 [64, 2048, 3072], P('ep', None, 'tp'), may hold values from -0.125 to 0.125
- down_weight: bfloat16 [64, 3072, 2048], P('ep', 'tp'), may hold values from -0.109375 to 0.109375
- expert_ids: int32 [16384, 2], P('ep'), may hold values from 0 to 63, all different within a row; in each aligned block of 256 rows (0 to 255, 256 to 511, ...) at most 16 rows name the same one
- route_weight: float32 [16384, 2], P('ep'), may hold values from 0.2 to 1
Outputs:
- mixer_out: bfloat16 [32768, 2048], P(('ep', 'tp'))
- expert_out: bfloat16 [16384, 2048], P('ep', 'tp')
Inputs may be any that keep to these rules, and one draw needn't show every extreme that they name: `expert_ids`: each row names 2 different experts. In the rows of one device no expert is named by more than 16 rows; the bound is reached at some expert in some device's rows.
All inputs are finite; a program needn't handle non-finite values.
Results may differ from a plain program's by a relative error of at most 0.012.
Values may be sent and summed in bfloat16 or wider, within the bound.
A program may use at most 64 MiB of HBM per device.

v0:
```python
import jax
import jax.numpy as jnp
from jax import lax
from jax.sharding import PartitionSpec as P

eps_rms = 1e-06
eps_norm = 1e-05


def from_behind(value, axis, by):
    count = lax.axis_size(axis)
    pairs = [(i, i + by) for i in range(count) if 0 <= i + by < count]
    return lax.ppermute(value, axis, pairs)


def slot_numbers(expert_ids, experts, capacity):
    chosen = expert_ids.reshape(-1)
    onehot = (chosen[:, None] == jnp.arange(experts, dtype=jnp.int32)[None, :]).astype(jnp.int32)
    earlier = jnp.cumsum(onehot, axis=0) - onehot
    position = jnp.sum(earlier * onehot, axis=1)
    return chosen * capacity + position


def fill_slots(normed, slot_index, experts, capacity, chosen_per_token):
    owners = jnp.full((experts * capacity,), -1, jnp.int32)
    token_of = jnp.arange(slot_index.shape[0], dtype=jnp.int32) // chosen_per_token
    owners = owners.at[slot_index].set(token_of)
    picked = jnp.take(normed, jnp.maximum(owners, 0), axis=0)
    filled = jnp.where((owners >= 0)[:, None], picked, jnp.zeros_like(picked))
    return filled.reshape(experts, capacity, normed.shape[1])


def on_device(
    glu_value,
    glu_gate,
    conv_kernel,
    ln_gain,
    out_weight,
    moe_input,
    moe_gain,
    gate_weight,
    up_weight,
    down_weight,
    expert_ids,
    route_weight,
):
    length, channels_dev = glu_value.shape
    reach = conv_kernel.shape[0]
    tp_count = lax.axis_size("tp")
    gated = (glu_value.astype(jnp.float32) * jax.nn.sigmoid(glu_gate.astype(jnp.float32))).astype(
        jnp.bfloat16
    )
    earlier_rows = from_behind(gated[length - (reach - 1) :], "ep", 1)
    padded = jnp.concatenate([earlier_rows, gated], axis=0).astype(jnp.float32)
    convolved = jnp.zeros((length, channels_dev), jnp.float32)
    for tap_index in range(reach):
        begin = reach - 1 - tap_index
        convolved = convolved + conv_kernel[tap_index] * padded[begin : begin + length]
    total, squares = lax.psum(
        (jnp.sum(convolved, axis=1), jnp.sum(convolved * convolved, axis=1)), "tp"
    )
    channels = channels_dev * tp_count
    mean = total / channels
    variance = squares / channels - mean * mean
    scaled = (convolved - mean[:, None]) * lax.rsqrt(variance + eps_norm)[:, None] * ln_gain
    activated = jax.nn.silu(scaled).astype(jnp.bfloat16)
    mixer_out = lax.psum_scatter(
        jnp.dot(activated, out_weight, preferred_element_type=jnp.float32).astype(jnp.bfloat16),
        "tp",
        scatter_dimension=0,
        tiled=True,
    )
    tokens, model_width = moe_input.shape
    chosen_per_token = expert_ids.shape[1]
    experts = lax.axis_size("ep")
    capacity = 4 * max(1, tokens // experts)
    values = moe_input.astype(jnp.float32)
    normed = (
        values * lax.rsqrt(jnp.mean(values * values, axis=1, keepdims=True) + eps_rms) * moe_gain
    ).astype(jnp.bfloat16)
    slot_index = slot_numbers(expert_ids, experts, capacity)
    outgoing = fill_slots(normed, slot_index, experts, capacity, chosen_per_token)
    w_gate = gate_weight[0]
    w_up = up_weight[0]
    w_down = down_weight[0]
    quarter_slots = capacity // tp_count
    own_slots = lax.dynamic_slice_in_dim(
        outgoing, lax.axis_index("tp") * quarter_slots, quarter_slots, 1
    )
    arrived_part = lax.all_to_all(own_slots, "ep", split_axis=0, concat_axis=0, tiled=True)
    arrived = lax.all_gather(arrived_part, "tp", axis=1, tiled=True)
    flattened = arrived.reshape(-1, model_width)
    gate_act = jnp.dot(flattened, w_gate, preferred_element_type=jnp.float32)
    up_act = jnp.dot(flattened, w_up, preferred_element_type=jnp.float32)
    hidden_rows = (jax.nn.silu(gate_act) * up_act).astype(jnp.bfloat16)
    hidden = hidden_rows.reshape(arrived.shape[0], arrived.shape[1], w_gate.shape[1])
    sources = hidden.shape[0]
    partial_sum = jnp.dot(
        hidden.reshape(-1, hidden.shape[2]), w_down, preferred_element_type=jnp.float32
    )
    partial_sum = partial_sum.reshape(sources, capacity, model_width)
    answers = lax.psum_scatter(
        partial_sum.astype(jnp.bfloat16), "tp", scatter_dimension=2, tiled=True
    )
    returned = lax.all_to_all(answers, "ep", split_axis=0, concat_axis=0, tiled=True)
    feature_dev = returned.shape[2]
    picked = jnp.take(returned.reshape(experts * capacity, feature_dev), slot_index, axis=0)
    picked = picked.astype(jnp.float32).reshape(tokens, chosen_per_token, feature_dev)
    expert_out = jnp.sum(picked * route_weight[:, :, None], axis=1).astype(jnp.bfloat16)
    return (mixer_out, expert_out)


def solution(mesh):
    in_specs = (
        P("ep", "tp"),
        P("ep", "tp"),
        P(None, "tp"),
        P("tp"),
        P("tp", None),
        P("ep", None),
        P(),
        P("ep", None, "tp"),
        P("ep", None, "tp"),
        P("ep", "tp", None),
        P("ep", None),
        P("ep", None),
    )
    out_specs = (P(("ep", "tp"), None), P("ep", "tp"))
    return jax.shard_map(
        on_device, mesh=mesh, in_specs=in_specs, out_specs=out_specs, check_vma=False
    )
```

profile of v0, /device:TPU:1, one launch (start us, length us, event | category | flops | bytes accessed | tf_op | source)
XLA Modules:
  0.0 243.3 jit_solution(11828817897513829075)
XLA Ops:
  7.2 0.0 all-gather.2.cloned.1.call-start
  7.2 1.0 copy.45
  8.2 0.1 eq.26
  8.3 0.1 reshape.105
  8.5 0.7 broadcast_multiply_fusion
  9.2 1.2 reduce-window.6
  10.4 0.2 slice_reduce_fusion
  10.7 0.1 copy.50
  10.8 0.1 mul.502
  11.0 0.1 fusion.47
  11.1 2.4 %scatter_custom_fusion = s32[1024]{0:T(1024)S(1)} fusion(s32[512]{0:T(512)S(1)} %bitcast.76, s32[512]{0:T(512)S(1)} %add_select_fusion, s32[]{:T(128)} %constant.76.clone.1), kind=kCustom, calls=%fused_computation.111 | custom fusion | bytes 4100 | tf_op jit(solution)/shard_map/scatter | solution.py:27
  13.6 0.1 broadcast_in_dim.51
  13.7 0.1 broadcast_in_dim.53
  13.8 1.5 fusion.7
  15.3 2.5 %fusion.9 = bf16[256,2048]{1,0:T(8,128)(2,1)} fusion(bf16[256,2048]{1,0:T(8,128)(2,1)} %param.17, f32[2048]{0:T(1024)} %param.18, f32[256]{0:T(256)S(1)} %add_rsqrt_fusion.1), kind=kLoop, calls=%fused_computation.15 | loop fusion | flops 2097152 | bytes 2106368 | tf_op jit(solution)/shard_map/convert_element_type | solution.py:80
  17.8 10.2 %gather_fusion = bf16[1024,2048]{1,0:T(8,128)(2,1)} fusion(bf16[256,2048]{1,0:T(8,128)(2,1)} %fusion.9, s32[1024]{0:T(1024)S(1)} %maximum_clamp_fusion), kind=kCustom, calls=%fused_computation | custom fusion | bytes 8392704 | tf_op jit(solution)/shard_map/jit(_take)/gather | solution.py:28
  28.0 0.1 constant_dynamic-slice_fusion
  28.1 2.5 %fusion.10 = bf16[64,4,2048]{2,1,0:T(4,128)(2,1)S(1)} fusion(bf16[64,16,2048]{2,1,0:T(8,128)(2,1)} %bitcast.72, s32[]{:T(128)S(6)} %select_n.48, pred[64,4]{1,0:T(8,128)(4,1)S(1)} %get-tuple-element.43, pred[64,4]{1,0:T(8,128)(4,1)S(1)} %get-tuple-element.42), kind=kLoop, calls=%fused_computation.17 | loop fusion | flops 1048576 | bytes 2097668 | tf_op jit(solution)/shard_map/jit(_where)/select_n | solution.py:29
  30.6 41.1 %all_to_all.10 = bf16[64,4,2048]{2,1,0:T(4,128)(2,1)S(1)} all-to-all(bf16[64,4,2048]{2,1,0:T(4,128)(2,1)S(1)} %fusion.10), channel_id=1, replica_groups=mesh['ep'=64,'tp'=4] {'ep'}, dimensions={0} | all-to-all | bytes 2097152 | tf_op jit(solution)/shard_map/all_to_all | solution.py:90
  71.7 1.6 copy.51
  73.2 0.0 all-gather.2.cloned.1.call-update
  73.3 0.2 reduce-scatter.5.cloned.1.call-start
  73.5 47.4 %all-gather.2.cloned.1.call-done = bf16[64,16,2048]{2,0,1:T(8,128)(2,1)} async-done(((bf16[64,4,2048]{2,0,1:T(8,128)(2,1)}), bf16[64,16,2048]{2,0,1:T(8,128)(2,1)}) %all-gather.2.cloned.1.call-update) | async-done | bytes 4194320 | tf_op jit(solution)/shard_map/all_gather | solution.py:91
  120.9 4.6 %copy.52 = bf16[64,16,2048]{2,1,0:T(8,128)(2,1)S(1)} copy(bf16[64,16,2048]{2,0,1:T(8,128)(2,1)} %all-gather.2.cloned.1.call-done) | data formatting | bytes 8388608 | tf_op jit(solution)/shard_map/all_gather | solution.py:91
  125.5 3.4 %fusion.1 = f32[1024,768]{1,0:T(8,128)S(1)} fusion(bf16[1024,2048]{1,0:T(8,128)(2,1)S(1)} %bitcast.73, bf16[1,2048,768]{2,1,0:T(8,128)(2,1)S(1)} %copy-done.5), kind=kOutput, calls=%fused_computation.5 | convolution fusion | flops 3221225472 | bytes 10485760 | tf_op jit(solution)/shard_map/dot_general | solution.py:94
  129.0 3.7 %multiply_convert_fusion = bf16[1024,768]{1,0:T(8,128)(2,1)S(1)} fusion(f32[1024,768]{1,0:T(8,128)S(1)} %fusion.1, bf16[1024,2048]{1,0:T(8,128)(2,1)S(1)} %bitcast.74, bf16[1,2048,768]{2,1,0:T(8,128)(2,1)S(1)} %copy-done.6), kind=kOutput, calls=%fused_computation.9 | convolution fusion | flops 3225944064 | bytes 12058624 | tf_op jit(solution)/shard_map/dot_general | solution.py:93
  132.7 5.0 %convolution_convert_fusion = bf16[64,16,2048]{2,1,0:T(8,128)(2,1)} fusion(bf16[64,16,768]{2,1,0:T(8,128)(2,1)S(1)} %bitcast.109, bf16[1,768,2048]{2,1,0:T(8,128)(2,1)S(1)} %copy-done), kind=kOutput, calls=%fused_computation.3 | convolution fusion | flops 3223322624 | bytes 8912896 | tf_op jit(solution)/shard_map/dot_general | solution.py:98
  137.7 0.0 reduce-scatter.5.cloned.1.call-update
  137.8 0.0 reduce-scatter.3.cloned.1.call-start
  137.8 0.9 copy-done.1
  138.7 1.1 multiply_convert_fusion.2
  139.8 3.8 %collective-permute-start = (bf16[30,256]{1,0:T(8,128)(2,1)S(1)}, bf16[30,256]{1,0:T(8,128)(2,1)S(1)}, u32[]{:S(2)}, u32[]{:S(2)}) collective-permute-start(bf16[30,256]{1,0:T(8,128)(2,1)S(1)} %slice.264), channel_id=1, source_target_pairs={{0,4},{4,8},{8,12},{12,16},{16,20},{20,24},{24,28},{28,32},{32,36}... | collective-permute-start | bytes 46088 | tf_op jit(solution)/shard_map/ppermute | solution.py:13
  143.7 0.8 collective-permute-done
  144.5 0.1 maximum_convert_fusion
  144.6 2.9 %fusion.55 = (f32[512]{0:T(512)S(1)}, f32[512]{0:T(512)S(1)}, f32[512,256]{1,0:T(8,128)}) fusion(f32[542,256]{1,0:T(8,128)S(1)} %maximum_convert_fusion, f32[256]{0:T(256)S(1)} %bitcast.107, f32[256]{0:T(256)S(1)} %bitcast.108, f32[256]{0:T(256)S(1)} %bitcast.79, f32[256]{0:T(256)S(1)} %bitcast.80, f32[256]{0:T(256)S(1)} %bitcast.81, f32[256]{0:T(256)S(1)} %bitcast.82, ...), kind=kLoop, calls=%fused_computation.121 | loop fusion | flops 8387584 | bytes 16813056 | tf_op jit(solution)/shard_map/reduce_sum | solution.py:60
  147.5 7.3 %all-reduce = (f32[512]{0:T(512)S(1)}, f32[512]{0:T(512)S(1)}) all-reduce(f32[512]{0:T(512)S(1)} %get-tuple-element.3, f32[512]{0:T(512)S(1)} %get-tuple-element.2), channel_id=1, replica_groups=mesh['ep'=64,'tp'=4] {'tp'}, use_global_device_ids=true, to_apply=%region_3.0 | all-reduce | flops 1024 | bytes 8192 | tf_op jit(solution)/shard_map/psum | solution.py:59
  154.8 3.5 %convolution_convert_fusion.1 = bf16[512,2048]{1,0:T(8,128)(2,1)} fusion(bf16[256,2048]{1,0:T(8,128)(2,1)} %param.16, f32[512,256]{1,0:T(8,128)} %get-tuple-element.6, f32[256]{0:T(256)S(1)} %copy-done.7, f32[512]{0:T(512)S(1)} %get-tuple-element.41, f32[512]{0:T(512)S(1)} %get-tuple-element.40), kind=kOutput, calls=%fused_computation.10 | convolution fusion | flops 538968064 | bytes 3675136 | tf_op jit(solution)/shard_map/dot_general | solution.py:68
  158.4 0.0 reduce-scatter.3.cloned.1.call-update
  158.4 29.4 %reduce-scatter.5.cloned.1.call-done = bf16[64,16,512]{2,1,0:T(8,128)(2,1)} async-done(((bf16[64,16,2048]{2,1,0:T(8,128)(2,1)}), bf16[64,16,512]{2,1,0:T(8,128)(2,1)}) %reduce-scatter.5.cloned.1.call-update) | async-done | bytes 1048592 | tf_op jit(solution)/shard_map/reduce_scatter | solution.py:102
  187.8 11.0 %all-to-all-start.1 = ((bf16[64,16,512]{2,1,0:T(8,128)(2,1)}), bf16[64,16,512]{2,1,0:T(8,128)(2,1)}, u32[]{:S(2)}, u32[]{:S(2)}) async-start(bf16[64,16,512]{2,1,0:T(8,128)(2,1)} %reduce-scatter.5.cloned.1.call-done), calls=%async_computation.3 | async-start | bytes 2097152 | tf_op jit(solution)/shard_map/all_to_all | solution.py:105
  198.8 0.1 reduce_sum.52
  199.0 0.1 copy.48
  199.1 0.2 copy.49
  199.3 0.1 copy.53
  199.4 27.5 %all-to-all-done.1 = bf16[64,16,512]{2,1,0:T(8,128)(2,1)} async-done(((bf16[64,16,512]{2,1,0:T(8,128)(2,1)}), bf16[64,16,512]{2,1,0:T(8,128)(2,1)}, u32[]{:S(2)}, u32[]{:S(2)}) %all-to-all-start.1) | async-done | bytes 1048608 | tf_op jit(solution)/shard_map/all_to_all | solution.py:105
  226.9 4.0 %gather_fusion.1 = bf16[512,512]{1,0:T(8,128)(2,1)} fusion(bf16[1024,512]{1,0:T(8,128)(2,1)} %bitcast.41, s32[1024]{0:T(1024)S(1)} %pad_clamp_fusion), kind=kCustom, calls=%fused_computation.1 | custom fusion | bytes 1050624 | tf_op jit(solution)/shard_map/jit(_take)/gather | solution.py:107
  230.9 2.0 gather.15
  232.9 3.9 %multiply_reduce_fusion = bf16[256,512]{1,0:T(8,128)(2,1)} fusion(bf16[256,2,512]{2,1,0:T(2,128)(2,1)} %gather.15, pred[256,2]{1,0:T(8,128)(4,1)S(1)} %copy.49, f32[256,2]{1,0:T(8,128)S(1)} %copy.53), kind=kLoop, calls=%fused_computation.18 | loop fusion | flops 917504 | bytes 788992 | tf_op jit(solution)/shard_map/reduce_sum | solution.py:109
  (30 shorter events, 0.2 us)
Async XLA Ops:
  7.2 125.6 %copy-start = (bf16[1,768,2048]{2,1,0:T(8,128)(2,1)S(1)}, bf16[1,768,2048]{2,1,0:T(8,128)(2,1)}, u32[]{:S(2)}) copy-start(bf16[1,768,2048]{2,1,0:T(8,128)(2,1)} %param.21) | copy-start | bytes 9437188
  7.2 113.7 %all-gather.2.cloned.1.call-start = ((), (), s32[]{:S(2)}) async-start(), calls=%async_computation.5 | async-start | bytes 5242880 | tf_op jit(solution)/shard_map/all_gather | solution.py:91
  73.3 114.6 %reduce-scatter.5.cloned.1.call-start = ((), (), s32[]{:S(2)}) async-start(), calls=%async_computation.6 | async-start | bytes 5242880 | tf_op jit(solution)/shard_map/reduce_scatter | solution.py:102
  120.9 4.6 %copy-start.5 = (bf16[1,2048,768]{2,1,0:T(8,128)(2,1)S(1)}, bf16[1,2048,768]{2,1,0:T(8,128)(2,1)}, u32[]{:S(2)}) copy-start(bf16[1,2048,768]{2,1,0:T(8,128)(2,1)} %param.20) | copy-start | bytes 9437188
  125.5 3.5 %copy-start.6 = (bf16[1,2048,768]{2,1,0:T(8,128)(2,1)S(1)}, bf16[1,2048,768]{2,1,0:T(8,128)(2,1)}, u32[]{:S(2)}) copy-start(bf16[1,2048,768]{2,1,0:T(8,128)(2,1)} %param.19) | copy-start | bytes 9437188
  137.7 0.9 copy-start.1
  137.7 5.9 %copy-start.2 = (f32[31,256]{1,0:T(8,128)S(1)}, f32[31,256]{1,0:T(8,128)}, u32[]{:S(2)}) copy-start(f32[31,256]{1,0:T(8,128)} %param.14) | copy-start | bytes 95236
  137.8 99.1 %reduce-scatter.3.cloned.1.call-start = ((), (), s32[]{:S(2)}) async-start(), calls=%async_computation.4 | async-start | bytes 2621440 | tf_op jit(solution)/shard_map/reduce_scatter | solution.py:67
  139.8 4.7 %collective-permute-start = (bf16[30,256]{1,0:T(8,128)(2,1)S(1)}, bf16[30,256]{1,0:T(8,128)(2,1)S(1)}, u32[]{:S(2)}, u32[]{:S(2)}) collective-permute-start(bf16[30,256]{1,0:T(8,128)(2,1)S(1)} %slice.264), channel_id=1, source_target_pairs={{0,4},{4,8},{8,12},{12,16},{16,20},{20,24},{24,28},{28,32},{32,36}... | collective-permute-start | bytes 46088 | tf_op jit(solution)/shard_map/ppermute | solution.py:13
  144.5 10.3 %copy-start.7 = (f32[256]{0:T(256)S(1)}, f32[256]{0:T(256)}, u32[]{:S(2)}) copy-start(f32[256]{0:T(256)} %param.15) | copy-start | bytes 3076
  158.4 40.7 %copy-start.3 = (s32[256,2]{0,1:T(2,128)S(1)}, s32[256,2]{0,1:T(2,128)}, u32[]{:S(2)}) copy-start(s32[256,2]{0,1:T(2,128)} %param.22) | copy-start | bytes 6148
  158.4 40.9 %copy-start.4 = (f32[256,2]{0,1:T(2,128)S(1)}, f32[256,2]{0,1:T(2,128)}, u32[]{:S(2)}) copy-start(f32[256,2]{0,1:T(2,128)} %param.23) | copy-start | bytes 6148
  187.8 39.1 %all-to-all-start.1 = ((bf16[64,16,512]{2,1,0:T(8,128)(2,1)}), bf16[64,16,512]{2,1,0:T(8,128)(2,1)}, u32[]{:S(2)}, u32[]{:S(2)}) async-start(bf16[64,16,512]{2,1,0:T(8,128)(2,1)} %reduce-scatter.5.cloned.1.call-done), calls=%async_computation.3 | async-start | bytes 2097152 | tf_op jit(solution)/shard_map/all_to_all | solution.py:105
Sparse Core Ops, SparseCore 0:
  73.4 47.4 all-gather.1
  137.9 49.9 reduce-scatter.4
  191.0 31.9 reduce-scatter.2
where the time goes:
time: 244 us; the launch traced here: 243 us
  waiting for transfers between devices  105 us (43%)
  blocking collectives  48.5 us (20%)
  local copies, waits for them, and re-layouts  28.4 us (12%)
  other arithmetic  16.6 us (7%)
  matrix products  15.7 us (6%)
  starting transfers between devices  15.1 us (6%)
  between operations  14 us (6%)
    all_gather x1, waiting for transfers between devices, on_device(): arrived = lax.all_gather(arrived_part, 'tp', axis=1, tiled=True)  47.4 us
    all_to_all x1, blocking collectives, on_device(): lax.all_to_all(own_slots, 'ep', split_axis=0, concat_axis=0, tiled=True)  41.1 us
    reduce_scatter x1, waiting for transfers between devices, on_device(): lax.psum_scatter(partial_sum.astype(jnp.bfloat16), 'tp', scatter_dimensio...  29.4 us
    all_to_all x1, waiting for transfers between devices, on_device(): lax.all_to_all(answers, 'ep', split_axis=0, concat_axis=0, tiled=True)  27.5 us
    all_to_all x1, starting transfers between devices, on_device(): lax.all_to_all(answers, 'ep', split_axis=0, concat_axis=0, tiled=True)  11 us
    gather x1, local copies, waits for them, and re-layouts, fill_slots(): picked = jnp.take(normed, jnp.maximum(owners, 0), axis=0)  10.2 us
    psum x1, blocking collectives, on_device(): lax.psum((jnp.sum(convolved, axis=1), jnp.sum(convolved * convolved, axis...  7.35 us
    gather x2, local copies, waits for them, and re-layouts, on_device(): jnp.take(returned.reshape(experts * capacity, feature_dev), slot_index, a...  6.05 us
  transfers between devices with their start and end apart: 5, of which 4 were waited for; matrix products, arithmetic and copies ran while one was open for 7% of the time, Pallas kernels for 0%

commit v1 on v0

v1 whole, which is shorter than its diff:
```python
import functools

import jax
import jax.numpy as jnp
from jax import lax
from jax.experimental import pallas as pl
from jax.experimental.pallas import tpu as pltpu
from jax.sharding import PartitionSpec as P

eps_rms = 1e-06
eps_norm = 1e-05
MESH = pl.DeviceIdType.MESH
F32 = jnp.float32
BF16 = jnp.bfloat16

A2A_S, A2A_R, AGR_S, AGR_R, AGL_S, AGL_R, FWR_S, FWR_R, FWL_S, FWL_R = range(10)
S1R_S, S1R_R, S1L_S, S1L_R, S2R_S, S2R_R, S2L_S, S2L_R, RET_S, RET_R = range(10, 20)


def layout_of(ep_count):
    if ep_count == 64:
        return 8, (0, 7, 1, 4, 3, 5, 2, 6), 2
    return 2, tuple(range(ep_count // 2)), 1


def from_behind(value, axis, by):
    count = lax.axis_size(axis)
    pairs = [(i, i + by) for i in range(count) if 0 <= i + by < count]
    return lax.ppermute(value, axis, pairs)


def moe_kernel(
    cfg,
    moe_in,
    gain,
    ids,
    ids_t,
    route,
    w_gate_hbm,
    w_up_hbm,
    w_down_hbm,
    out,
    wg,
    wu,
    wd,
    normed,
    send_full,
    send_part,
    xin,
    hid,
    part,
    s1r,
    s1l,
    s2r,
    s2l,
    ans,
    ret,
    w_sem,
    sems,
):
    nz, nyc, order, per_chunk, cap = cfg
    ep = lax.axis_index("ep")
    x = lax.axis_index("tp")
    z = ep // nyc
    yc = ep % nyc
    xp, xm, xo = (x + 1) % 4, (x + 3) % 4, (x + 2) % 4
    n_ep = nz * nyc
    n_chunks = nz // per_chunk
    rows = per_chunk * nyc * cap
    half = rows // 2
    group = nyc * cap
    tokens, width = moe_in.shape
    quarter = width // 4

    barrier = pltpu.get_barrier_semaphore()

    def greet(j, c):
        pl.semaphore_signal(
            barrier, inc=1, device_id=((ep + j) % n_ep, x), device_id_type=MESH
        )
        return c

    lax.fori_loop(1, n_ep, greet, 0)
    for other in (xp, xm):
        pl.semaphore_signal(barrier, inc=1, device_id=(ep, other), device_id_type=MESH)

    loads = [
        pltpu.make_async_copy(w_gate_hbm.at[0], wg, w_sem.at[0]),
        pltpu.make_async_copy(w_up_hbm.at[0], wu, w_sem.at[1]),
        pltpu.make_async_copy(w_down_hbm.at[0], wd, w_sem.at[2]),
    ]
    for load in loads:
        load.start()

    def rdma(src, dst, row_s, row_r, k, to_ep, to_x):
        return pltpu.make_async_remote_copy(
            src_ref=src,
            dst_ref=dst,
            send_sem=sems.at[row_s, k],
            recv_sem=sems.at[row_r, k],
            device_id=(to_ep, to_x),
            device_id_type=MESH,
        )

    block = min(32, tokens)

    def norm_rows(i, c):
        at = pl.ds(pl.multiple_of(i * block, block), block)
        v = moe_in[at, :].astype(F32)
        scale = lax.rsqrt(jnp.sum(v * v, axis=1, keepdims=True) / width + eps_rms)
        y = (v * scale * gain[...]).astype(BF16)
        for q in range(4):
            normed[q, at, :] = y[:, q * quarter : (q + 1) * quarter]
        return c

    lax.fori_loop(0, tokens // block, norm_rows, 0)

    def place(e):
        dz = (e // nyc - z + nz) % nz
        pos = jnp.zeros_like(e)
        for p, d in enumerate(order):
            pos = jnp.where(dz == d, p, pos)
        return ((pos * nyc + e % nyc) * cap).astype(F32)

    ti = lax.broadcasted_iota(jnp.int32, (tokens, tokens), 0)
    tj = lax.broadcasted_iota(jnp.int32, (tokens, tokens), 1)
    er = lax.broadcasted_iota(jnp.int32, (64, tokens), 0)
    e0r, e1r = ids_t[0:1, :], ids_t[1:2, :]
    m0r, m1r = er == e0r, er == e1r
    mbr = jnp.where(m0r | m1r, 1.0, 0.0).astype(BF16)
    before = jnp.where(ti < tj, 1.0, 0.0).astype(BF16)
    earlier_r = jnp.dot(mbr, before, preferred_element_type=F32)
    slot0r = place(e0r) + jnp.sum(jnp.where(m0r, earlier_r, 0.0), axis=0, keepdims=True)
    slot1r = place(e1r) + jnp.sum(jnp.where(m1r, earlier_r, 0.0), axis=0, keepdims=True)

    def pick_rows(start, count):
        at = (lax.broadcasted_iota(jnp.int32, (count, tokens), 0) + start).astype(F32)
        return jnp.where((at == slot0r) | (at == slot1r), 1.0, 0.0).astype(BF16)

    for p in range(per_chunk):
        pick = pick_rows(p * group, group)
        for q in range(4):
            send_full[q, p * group : (p + 1) * group, :] = jnp.dot(
                pick, normed[q], preferred_element_type=F32
            ).astype(BF16)

    def fill_part(p, c):
        pick = pick_rows((p + per_chunk) * group, group)
        at = pl.ds(pl.multiple_of(p * group, group), group)
        send_part[at, :] = jnp.dot(pick, normed[x], preferred_element_type=F32).astype(BF16)
        return c

    lax.fori_loop(0, nz - per_chunk, fill_part, 0)

    pl.semaphore_wait(barrier, n_ep - 1 + 2)

    for p in range(nz):
        dz = order[p]
        k = p // per_chunk
        to_z = (z + dz) % nz

        def send(j, c, p=p, dz=dz, k=k, to_z=to_z):
            other = (yc + j) % nyc
            there = pl.ds(pl.multiple_of((p * nyc + yc) * cap, cap), cap)
            if k == 0:
                here = pl.ds(pl.multiple_of((p * nyc + other) * cap, cap), cap)
                copy = rdma(
                    send_full.at[:, here, :],
                    xin.at[:, there, :],
                    A2A_S, A2A_R, k, to_z * nyc + other, x,
                )
            else:
                here = pl.ds(
                    pl.multiple_of(((p - per_chunk) * nyc + other) * cap, cap), cap
                )
                copy = rdma(
                    send_part.at[here, :],
                    xin.at[x, there, :],
                    A2A_S, A2A_R, k, to_z * nyc + other, x,
                )
            copy.start()
            return c

        lax.fori_loop(1 if dz == 0 else 0, nyc, send, 0)

    mine = pl.ds(pl.multiple_of(yc * cap, cap), cap)
    for q in range(4):
        xin[q, mine, :] = send_full[q, mine, :]

    ec = lax.broadcasted_iota(jnp.int32, (tokens, 128), 1)
    e0c, e1c = ids[:, 0:1], ids[:, 1:2]
    m0c, m1c = ec == e0c, ec == e1c
    mbc = jnp.where(m0c | m1c, 1.0, 0.0).astype(BF16)
    after = jnp.where(tj < ti, 1.0, 0.0).astype(BF16)
    earlier_c = jnp.dot(after, mbc, preferred_element_type=F32)
    slot0c = place(e0c) + jnp.sum(jnp.where(m0c, earlier_c, 0.0), axis=1, keepdims=True)
    slot1c = place(e1c) + jnp.sum(jnp.where(m1c, earlier_c, 0.0), axis=1, keepdims=True)

    for load in loads:
        load.wait()

    def at_chunk(k):
        return pl.ds(k * rows, rows)

    def wait_in(k):
        if k == 0:
            region = xin.at[:, pl.ds(0, rows - cap), :]
        else:
            region = xin.at[x, at_chunk(k), :]
        rdma(region, region, A2A_S, A2A_R, k, ep, xp).wait_recv()

    def gather_start(k):
        region = xin.at[x, at_chunk(k), :]
        rdma(region, region, AGR_S, AGR_R, k, ep, xp).start()
        rdma(region, region, AGL_S, AGL_R, k, ep, xm).start()

    def gather_forward(k):
        left = xin.at[xm, at_chunk(k), :]
        rdma(left, left, AGR_S, AGR_R, k, ep, xp).wait_recv()
        top = xin.at[xm, pl.ds(k * rows, half), :]
        rdma(top, top, FWR_S, FWR_R, k, ep, xp).start()
        right = xin.at[xp, at_chunk(k), :]
        rdma(right, right, AGL_S, AGL_R, k, ep, xm).wait_recv()
        low = xin.at[xp, pl.ds(k * rows + half, half), :]
        rdma(low, low, FWL_S, FWL_R, k, ep, xm).start()

    def gather_done(k):
        top = xin.at[xo, pl.ds(k * rows, half), :]
        low = xin.at[xo, pl.ds(k * rows + half, half), :]
        rdma(top, top, FWR_S, FWR_R, k, ep, xp).wait_recv()
        rdma(low, low, FWL_S, FWL_R, k, ep, xm).wait_recv()

    hidden_dev = wg.shape[1]
    nb = min(256, hidden_dev)

    def compute(k):
        def up(n, c):
            cols = pl.ds(pl.multiple_of(n * nb, nb), nb)
            g = jnp.zeros((rows, nb), F32)
            u = jnp.zeros((rows, nb), F32)
            for q in range(4):
                xq = xin[q, at_chunk(k), :]
                ws = pl.ds(q * quarter, quarter)
                g = g + jnp.dot(xq, wg[ws, cols], preferred_element_type=F32)
                u = u + jnp.dot(xq, wu[ws, cols], preferred_element_type=F32)
            hid[:, cols] = (g / (1.0 + jnp.exp(-g)) * u).astype(BF16)
            return c

        lax.fori_loop(0, hidden_dev // nb, up, 0)

        def down(d):
            cols = pl.ds(pl.multiple_of(d * quarter, quarter), quarter)
            part[k, d] = jnp.dot(
                hid[...], wd[:, cols], preferred_element_type=F32
            ).astype(BF16)

        down(xo)
        down(xp)
        rdma(
            part.at[k, xo, pl.ds(0, half), :], s1r.at[k], S1R_S, S1R_R, k, ep, xp
        ).start()
        rdma(
            part.at[k, xo, pl.ds(half, half), :], s1l.at[k], S1L_S, S1L_R, k, ep, xm
        ).start()
        down(xm)
        down(x)

    def scatter_add(k):
        rdma(s1r.at[k], s1r.at[k], S1R_S, S1R_R, k, ep, xp).wait_recv()
        top = pl.ds(0, half)
        part[k, xp, top, :] = (
            part[k, xp, top, :].astype(F32) + s1r[k].astype(F32)
        ).astype(BF16)
        rdma(s1l.at[k], s1l.at[k], S1L_S, S1L_R, k, ep, xm).wait_recv()
        low = pl.ds(half, half)
        part[k, xm, low, :] = (
            part[k, xm, low, :].astype(F32) + s1l[k].astype(F32)
        ).astype(BF16)
        rdma(part.at[k, xp], s2r.at[k], S2R_S, S2R_R, k, ep, xp).start()
        rdma(part.at[k, xm], s2l.at[k], S2L_S, S2L_R, k, ep, xm).start()

    def give_back(k):
        rdma(s2r.at[k], s2r.at[k], S2R_S, S2R_R, k, ep, xp).wait_recv()
        rdma(s2l.at[k], s2l.at[k], S2L_S, S2L_R, k, ep, xm).wait_recv()
        total = part[k, x].astype(F32) + s2r[k].astype(F32) + s2l[k].astype(F32)
        ans[at_chunk(k), :] = total.astype(BF16)
        if k == 0:
            ret[mine, :] = ans[mine, :]
        for p in range(k * per_chunk, (k + 1) * per_chunk):
            dz = order[p]
            to_z = (z - dz + nz) % nz

            def send(j, c, p=p, to_z=to_z):
                other = (yc + j) % nyc
                here = pl.ds(pl.multiple_of((p * nyc + other) * cap, cap), cap)
                there = pl.ds(pl.multiple_of((p * nyc + yc) * cap, cap), cap)
                rdma(
                    ans.at[here, :], ret.at[there, :], RET_S, RET_R, k,
                    to_z * nyc + other, x,
                ).start()
                return c

            lax.fori_loop(1 if dz == 0 else 0, nyc, send, 0)

    wait_in(0)
    compute(0)
    if n_chunks > 1:
        wait_in(1)
        gather_start(1)
    for k in range(n_chunks):
        scatter_add(k)
        if k + 1 < n_chunks:
            gather_forward(k + 1)
        if k + 2 < n_chunks:
            wait_in(k + 2)
            gather_start(k + 2)
        if k + 1 < n_chunks:
            gather_done(k + 1)
            compute(k + 1)
        give_back(k)

    total = jnp.zeros((tokens, quarter), F32)
    w0, w1 = route[:, 0:1], route[:, 1:2]
    for k in range(n_chunks):
        count = rows - cap if k == 0 else rows
        region = ret.at[pl.ds(k * rows, count), :]
        rdma(region, region, RET_S, RET_R, k, ep, xp).wait_recv()
        at = (lax.broadcasted_iota(jnp.int32, (tokens, rows), 1) + k * rows).astype(F32)
        w = jnp.where(at == slot0c, w0, 0.0) + jnp.where(at == slot1c, w1, 0.0)
        high = w.astype(BF16)
        low = (w - high.astype(F32)).astype(BF16)
        got = ret[at_chunk(k), :]
        total = total + jnp.dot(high, got, preferred_element_type=F32)
        total = total + jnp.dot(low, got, preferred_element_type=F32)
    out[...] = total.astype(BF16)

    for k in range(n_chunks):
        if k == 0:
            region = send_full.at[:, pl.ds(0, rows - cap), :]
            back = ans.at[pl.ds(0, rows - cap), :]
        else:
            region = send_part.at[pl.ds((k - 1) * rows, rows), :]
            back = ans.at[at_chunk(k), :]
            whole = xin.at[x, at_chunk(k), :]
            part_half = xin.at[xm, pl.ds(k * rows, half), :]
            rdma(whole, whole, AGR_S, AGR_R, k, ep, xp).wait_send()
            rdma(whole, whole, AGL_S, AGL_R, k, ep, xm).wait_send()
            rdma(part_half, part_half, FWR_S, FWR_R, k, ep, xp).wait_send()
            rdma(part_half, part_half, FWL_S, FWL_R, k, ep, xm).wait_send()
        rdma(region, region, A2A_S, A2A_R, k, ep, xp).wait_send()
        rdma(s1r.at[k], s1r.at[k], S1R_S, S1R_R, k, ep, xp).wait_send()
        rdma(s1l.at[k], s1l.at[k], S1L_S, S1L_R, k, ep, xm).wait_send()
        rdma(s2r.at[k], s2r.at[k], S2R_S, S2R_R, k, ep, xp).wait_send()
        rdma(s2l.at[k], s2l.at[k], S2L_S, S2L_R, k, ep, xm).wait_send()
        rdma(back, back, RET_S, RET_R, k, ep, xp).wait_send()


def run_experts(moe_input, moe_gain, gate_weight, up_weight, down_weight, expert_ids, route_weight):
    tokens, width = moe_input.shape
    ep_count = lax.axis_size("ep")
    nyc, order, per_chunk = layout_of(ep_count)
    nz = ep_count // nyc
    cap = 16
    hidden_dev = gate_weight.shape[2]
    quarter = width // 4
    n_chunks = nz // per_chunk
    rows = per_chunk * nyc * cap
    slots = ep_count * cap
    vmem = pl.BlockSpec(memory_space=pltpu.VMEM)
    hbm = pl.BlockSpec(memory_space=pl.ANY)
    cfg = (nz, nyc, order, per_chunk, cap)
    return pl.pallas_call(
        functools.partial(moe_kernel, cfg),
        out_shape=jax.ShapeDtypeStruct((tokens, quarter), BF16),
        in_specs=[vmem] * 5 + [hbm] * 3,
        out_specs=vmem,
        scratch_shapes=[
            pltpu.VMEM((width, hidden_dev), BF16),
            pltpu.VMEM((width, hidden_dev), BF16),
            pltpu.VMEM((hidden_dev, width), BF16),
            pltpu.VMEM((4, tokens, quarter), BF16),
            pltpu.VMEM((4, rows, quarter), BF16),
            pltpu.VMEM((max(slots - rows, rows), quarter), BF16),
            pltpu.VMEM((4, slots, quarter), BF16),
            pltpu.VMEM((rows, hidden_dev), BF16),
            pltpu.VMEM((n_chunks, 4, rows, quarter), BF16),
            pltpu.VMEM((n_chunks, rows // 2, quarter), BF16),
            pltpu.VMEM((n_chunks, rows // 2, quarter), BF16),
            pltpu.VMEM((n_chunks, rows, quarter), BF16),
            pltpu.VMEM((n_chunks, rows, quarter), BF16),
            pltpu.VMEM((slots, quarter), BF16),
            pltpu.VMEM((slots, quarter), BF16),
            pltpu.SemaphoreType.DMA((3,)),
            pltpu.SemaphoreType.DMA((20, n_chunks)),
        ],
        compiler_params=pltpu.CompilerParams(
            collective_id=0, has_side_effects=True, vmem_limit_bytes=60 * 1024 * 1024
        ),
        cost_estimate=pl.CostEstimate(
            flops=10_000_000_000, bytes_accessed=12_000_000, transcendentals=0
        ),
        name="experts",
    )(
        moe_input,
        moe_gain[None, :],
        expert_ids,
        expert_ids.T,
        route_weight,
        gate_weight,
        up_weight,
        down_weight,
    )


def on_device(
    glu_value,
    glu_gate,
    conv_kernel,
    ln_gain,
    out_weight,
    moe_input,
    moe_gain,
    gate_weight,
    up_weight,
    down_weight,
    expert_ids,
    route_weight,
):
    length, channels_dev = glu_value.shape
    reach = conv_kernel.shape[0]
    tp_count = lax.axis_size("tp")
    gated = (glu_value.astype(F32) * jax.nn.sigmoid(glu_gate.astype(F32))).astype(BF16)
    earlier_rows = from_behind(gated[length - (reach - 1) :], "ep", 1)
    padded = jnp.concatenate([earlier_rows, gated], axis=0).astype(F32)
    convolved = jnp.zeros((length, channels_dev), F32)
    for tap_index in range(reach):
        begin = reach - 1 - tap_index
        convolved = convolved + conv_kernel[tap_index] * padded[begin : begin + length]
    total, squares = lax.psum(
        (jnp.sum(convolved, axis=1), jnp.sum(convolved * convolved, axis=1)), "tp"
    )
    channels = channels_dev * tp_count
    mean = total / channels
    variance = squares / channels - mean * mean
    scaled = (convolved - mean[:, None]) * lax.rsqrt(variance + eps_norm)[:, None] * ln_gain
    activated = jax.nn.silu(scaled).astype(BF16)
    partial_sum = jnp.dot(activated, out_weight, preferred_element_type=F32).astype(BF16)
    partial_sum, moe_input = lax.optimization_barrier((partial_sum, moe_input))
    mixer_out = lax.psum_scatter(partial_sum, "tp", scatter_dimension=0, tiled=True)
    expert_out = run_experts(
        moe_input, moe_gain, gate_weight, up_weight, down_weight, expert_ids, route_weight
    )
    return (mixer_out, expert_out)


def solution(mesh):
    in_specs = (
        P("ep", "tp"),
        P("ep", "tp"),
        P(None, "tp"),
        P("tp"),
        P("tp", None),
        P("ep", None),
        P(),
        P("ep", None, "tp"),
        P("ep", None, "tp"),
        P("ep", "tp", None),
        P("ep", None),
        P("ep", None),
    )
    out_specs = (P(("ep", "tp"), None), P("ep", "tp"))
    return jax.shard_map(
        on_device, mesh=mesh, in_specs=in_specs, out_specs=out_specs, check_vma=False
    )
```

time: 244 us -> 154 us (0.63)
  Pallas kernels: 0 us -> 114 us
  waiting for transfers between devices: 105 us -> 0.04 us
  blocking collectives: 48.5 us -> 8.77 us
  local copies, waits for them, and re-layouts: 28.4 us -> 5.3 us
  matrix products: 15.7 us -> 2.14 us
  other arithmetic: 16.6 us -> 3.71 us
  starting transfers between devices: 15.1 us -> 4.62 us
    pallas_call x0 -> x1, Pallas kernels: none -> 114 us  [run_experts(): pl.pallas_call(functools.partial(moe_kernel, cfg), out_shape=jax.ShapeDty...]
    all_gather x1 -> x0, waiting for transfers between devices: 47.4 us -> none  [on_device(): arrived = lax.all_gather(arrived_part, 'tp', axis=1, tiled=True)]
    all_to_all x1 -> x0, blocking collectives: 41.1 us -> none  [on_device(): lax.all_to_all(own_slots, 'ep', split_axis=0, concat_axis=0, tiled=True)]
    reduce_scatter x2 -> x1, waiting for transfers between devices: 29.4 us -> 0.02 us  [on_device(): lax.psum_scatter(partial_sum, 'tp', scatter_dimension=0, tiled=True)]
    all_to_all x1 -> x0, waiting for transfers between devices: 27.5 us -> none  [on_device(): lax.all_to_all(answers, 'ep', split_axis=0, concat_axis=0, tiled=True)]
    gather x3 -> x0, local copies, waits for them, and re-layouts: 16.2 us -> none  [the longest x1 10.2 us: fill_slots(): picked = jnp.take(normed, jnp.maximum(owners, 0), axis=0)]
    dot_general x4 -> x1, matrix products: 15.7 us -> 2.14 us  [on_device(): jnp.dot(activated, out_weight, preferred_element_type=F32).astype(BF16)]
    all_to_all x1 -> x0, starting transfers between devices: 11 us -> none  [on_device(): lax.all_to_all(answers, 'ep', split_axis=0, concat_axis=0, tiled=True)]
  transfers between devices with their start and end apart: 5 -> 2, of which waited for: 4 -> 0; matrix products, arithmetic and copies ran while one was open for 7% -> 2% of each run, Pallas kernels for 0% -> 75%
where the time goes in v1:
time: 154 us; the launch traced here: 152 us
  Pallas kernels  114 us (74%)
  between operations  14.1 us (9%)
  blocking collectives  8.77 us (6%)
  local copies, waits for them, and re-layouts  5.3 us (3%)
  starting transfers between devices  4.62 us (3%)
  other arithmetic  3.71 us (2%)
  matrix products  2.14 us (1%)
    pallas_call x1, Pallas kernels, run_experts(): pl.pallas_call(functools.partial(moe_kernel, cfg), out_shape=jax.ShapeDty...  114 us
    psum x1, blocking collectives, on_device(): lax.psum((jnp.sum(convolved, axis=1), jnp.sum(convolved * convolved, axis...  8.77 us
    ppermute x1, starting transfers between devices, from_behind(): return lax.ppermute(value, axis, pairs)  4.58 us
    unnamed x11, local copies, waits for them, and re-layouts  3.29 us
  transfers between devices with their start and end apart: 2, of which 0 were waited for; matrix products, arithmetic and copies ran while one was open for 2% of the time, Pallas kernels for 75%

profile of v1, /device:TPU:1, one launch (start us, length us, event | category | flops | bytes accessed | tf_op | source)
XLA Modules:
  0.0 152.3 jit_solution(2041716676147711110)
XLA Ops:
  7.2 0.0 copy-start
  7.2 0.0 reduce-scatter.2.cloned.1.call-start
  7.2 1.3 multiply_convert_fusion.1
  8.5 4.6 %collective-permute-start = (bf16[30,256]{1,0:T(8,128)(2,1)S(1)}, bf16[30,256]{1,0:T(8,128)(2,1)S(1)}, u32[]{:S(2)}, u32[]{:S(2)}) collective-permute-start(bf16[30,256]{1,0:T(8,128)(2,1)S(1)} %slice.252), channel_id=1, source_target_pairs={{0,4},{4,8},{8,12},{12,16},{16,20},{20,24},{24,28},{28,32},{32,36}... | collective-permute-start | bytes 46088 | tf_op jit(solution)/shard_map/ppermute | solution.py:29
  13.1 1.0 fusion.37
  14.1 1.0 fusion.38
  15.1 0.0 collective-permute-done
  15.1 0.1 maximum_convert_fusion
  15.2 0.0 copy-start.3
  15.2 2.4 %fusion.35 = (f32[512]{0:T(512)S(1)}, f32[512]{0:T(512)S(1)}, f32[512,256]{1,0:T(8,128)S(1)}) fusion(f32[542,256]{1,0:T(8,128)S(1)} %maximum_convert_fusion, f32[256]{0:T(256)S(1)} %bitcast.63, f32[256]{0:T(256)S(1)} %bitcast.64, f32[256]{0:T(256)S(1)} %bitcast.35, f32[256]{0:T(256)S(1)} %bitcast.36, f32[256]{0:T(256)S(1)} %bitcast.37, f32[256]{0:T(256)S(1)} %bitcast.38, ...), kind=kLoop, calls=%fused_computation.73 | loop fusion | flops 8387584 | bytes 16813056 | tf_op jit(solution)/shard_map/reduce_sum | solution.py:440
  17.6 8.8 %all-reduce = (f32[512]{0:T(512)S(1)}, f32[512]{0:T(512)S(1)}) all-reduce(f32[512]{0:T(512)S(1)} %get-tuple-element.7, f32[512]{0:T(512)S(1)} %get-tuple-element.6), channel_id=1, replica_groups=mesh['ep'=64,'tp'=4] {'tp'}, use_global_device_ids=true, to_apply=%region_3.0 | all-reduce | flops 1024 | bytes 8192 | tf_op jit(solution)/shard_map/psum | solution.py:439
  26.4 0.0 copy-done
  26.4 0.0 copy-done.3
  26.4 0.0 copy-start.2
  26.4 0.0 copy-start.1
  26.4 2.1 %convolution_convert_fusion = bf16[512,2048]{1,0:T(8,128)(2,1)} fusion(bf16[256,2048]{1,0:T(8,128)(2,1)S(1)} %copy-done, f32[512,256]{1,0:T(8,128)S(1)} %get-tuple-element.10, f32[256]{0:T(256)S(1)} %copy-done.3, f32[512]{0:T(512)S(1)} %get-tuple-element.43, f32[512]{0:T(512)S(1)} %get-tuple-element.42), kind=kOutput, calls=%fused_computation | convolution fusion | flops 538968064 | bytes 3675136 | tf_op jit(solution)/shard_map/dot_general | solution.py:447
  28.5 0.0 reduce-scatter.2.cloned.1.call-update
  28.6 0.0 copy-done.2
  28.6 0.8 copy.14.ids
  29.4 0.0 copy-done.1
  29.4 0.8 copy.15.route
  30.2 113.6 %experts.1 = bf16[256,512]{1,0:T(8,128)(2,1)} custom-call(bf16[256,2048]{1,0:T(8,128)(2,1)} %moe_in, f32[1,2048]{1,0:T(1,128)} %bitcast.66, s32[256,2]{1,0:T(8,128)} %copy.14.ids, s32[2,256]{1,0:T(2,128)} %bitcast.65, f32[256,2]{1,0:T(8,128)} %copy.15.route, bf16[1,2048,768]{2,1,0:T(8,128)(2,1)} %w_gate_hbm.1, bf16[1,2048,768]{2,1,0:T(8,128)(2,1)} %w_up_hbm.1, ...), custom_call_target="tpu_custom_call" | custom-call | flops 10000000000 | bytes 12000000 | tf_op jit(solution)/shard_map/experts/pallas_call | solution.py:372
  143.7 0.0 reduce-scatter.2.cloned.1.call-done
  143.8 1.7 %copy.17 = bf16[256,512]{1,0:T(8,128)(2,1)} copy(bf16[256,512]{1,0:T(8,128)(2,1)} %experts.1) | data formatting | bytes 524288
  (2 shorter events, 0.0 us)
Async XLA Ops:
  7.2 19.2 %copy-start = (bf16[256,2048]{1,0:T(8,128)(2,1)S(1)}, bf16[256,2048]{1,0:T(8,128)(2,1)}, u32[]{:S(2)}) copy-start(bf16[256,2048]{1,0:T(8,128)(2,1)} %param.16) | copy-start | bytes 3145732
  7.2 136.6 %reduce-scatter.2.cloned.1.call-start = ((), (), s32[]{:S(2)}) async-start(), calls=%async_computation.1 | async-start | bytes 2621440 | tf_op jit(solution)/shard_map/reduce_scatter | solution.py:449
  8.5 6.6 %collective-permute-start = (bf16[30,256]{1,0:T(8,128)(2,1)S(1)}, bf16[30,256]{1,0:T(8,128)(2,1)S(1)}, u32[]{:S(2)}, u32[]{:S(2)}) collective-permute-start(bf16[30,256]{1,0:T(8,128)(2,1)S(1)} %slice.252), channel_id=1, source_target_pairs={{0,4},{4,8},{8,12},{12,16},{16,20},{20,24},{24,28},{28,32},{32,36}... | collective-permute-start | bytes 46088 | tf_op jit(solution)/shard_map/ppermute | solution.py:29
  15.2 11.2 %copy-start.3 = (f32[256]{0:T(256)S(1)}, f32[256]{0:T(256)}, u32[]{:S(2)}) copy-start(f32[256]{0:T(256)} %param.15) | copy-start | bytes 3076
  26.4 2.2 %copy-start.2 = (s32[256,2]{0,1:T(2,128)S(1)}, s32[256,2]{0,1:T(2,128)}, u32[]{:S(2)}) copy-start(s32[256,2]{0,1:T(2,128)} %param.22) | copy-start | bytes 6148
  26.4 3.0 %copy-start.1 = (f32[256,2]{0,1:T(2,128)S(1)}, f32[256,2]{0,1:T(2,128)}, u32[]{:S(2)}) copy-start(f32[256,2]{0,1:T(2,128)} %param.23) | copy-start | bytes 6148
Sparse Core Ops, SparseCore 0:
  28.7 34.6 reduce-scatter.1

commit v2 on v1

v2 whole, which is shorter than its diff:
```python
import functools

import jax
import jax.numpy as jnp
from jax import lax
from jax.experimental import pallas as pl
from jax.experimental.pallas import tpu as pltpu
from jax.sharding import PartitionSpec as P

eps_rms = 1e-06
eps_norm = 1e-05
MESH = pl.DeviceIdType.MESH
F32 = jnp.float32
BF16 = jnp.bfloat16

A2A_S, A2A_R, AGR_S, AGR_R, AGL_S, AGL_R, FWR_S, FWR_R, FWL_S, FWL_R = range(10)
S1R_S, S1R_R, S1L_S, S1L_R, S2R_S, S2R_R, S2L_S, S2L_R, RET_S, RET_R = range(10, 20)
A2P_S, A2P_R = 20, 21
HALO, STAT_P, STAT_M, STAT_O, ACT_P, ACT_M, ACT_O, WR, WL, WFR, WFL, WC_P, WC_M, WC_O = range(14)


def layout_of(ep_count):
    if ep_count == 64:
        return 8, (5, 3, 6, 4, 7, 2, 0, 1), (0, 0, 0, 0, 1, 1, 1, 1), 2
    return 2, (2, 3, 1, 0), (0, 0, 1, 1), 1


def block_kernel(
    cfg,
    gain,
    ids_t,
    route_t,
    taps,
    ln_gain,
    moe_hbm,
    value_hbm,
    gate_hbm,
    w_out_hbm,
    w_gate_hbm,
    w_up_hbm,
    w_down_hbm,
    mixed,
    out,
    moe_in,
    value,
    gate,
    w_out,
    wg,
    wu,
    wd,
    normed,
    send_full,
    send_part,
    xin,
    hid,
    part,
    s1r,
    s1l,
    s2r,
    s2l,
    ans,
    ret,
    tail,
    halo,
    gated,
    conv,
    stat,
    stat_in,
    act,
    act_in,
    total,
    w_sem,
    sems,
    msend,
    mrecv,
):
    nz, nyc, order, whole, per_chunk, cap = cfg
    ep = lax.axis_index("ep")
    x = lax.axis_index("tp")
    z = ep // nyc
    yc = ep % nyc
    xp, xm, xo = (x + 1) % 4, (x + 3) % 4, (x + 2) % 4
    n_ep = nz * nyc
    n_chunks = nz // per_chunk
    rows = per_chunk * nyc * cap
    half = rows // 2
    group = nyc * cap
    tokens, width = moe_in.shape
    quarter = width // 4
    whole_at = {p: sum(whole[:p]) for p in range(nz) if whole[p]}
    part_at = {p: p - sum(whole[:p]) for p in range(nz) if not whole[p]}
    own = order.index(0)

    barrier = pltpu.get_barrier_semaphore()

    def greet(j, c):
        pl.semaphore_signal(
            barrier, inc=1, device_id=((ep + j) % n_ep, x), device_id_type=MESH
        )
        return c

    lax.fori_loop(1, n_ep, greet, 0)
    for other in (xp, xm, xo):
        pl.semaphore_signal(barrier, inc=1, device_id=(ep, other), device_id_type=MESH)

    loads = [
        pltpu.make_async_copy(src, dst, w_sem.at[i])
        for i, (src, dst) in enumerate(
            (
                (moe_hbm, moe_in),
                (value_hbm, value),
                (gate_hbm, gate),
                (w_out_hbm, w_out.at[x]),
                (w_gate_hbm.at[0], wg),
                (w_up_hbm.at[0], wu),
                (w_down_hbm.at[0], wd),
            )
        )
    ]
    for load in loads:
        load.start()

    def rdma(src, dst, row_s, row_r, k, to_ep, to_x):
        return pltpu.make_async_remote_copy(
            src_ref=src,
            dst_ref=dst,
            send_sem=sems.at[row_s, k],
            recv_sem=sems.at[row_r, k],
            device_id=(to_ep, to_x),
            device_id_type=MESH,
        )

    block = min(32, tokens)

    def norm_rows(i, c):
        at = pl.ds(pl.multiple_of(i * block, block), block)
        v = moe_in[at, :].astype(F32)
        scale = lax.rsqrt(jnp.sum(v * v, axis=1, keepdims=True) / width + eps_rms)
        y = (v * scale * gain[...]).astype(BF16)
        for q in range(4):
            normed[q, at, :] = y[:, q * quarter : (q + 1) * quarter]
        return c

    def place(e):
        dz = (e // nyc - z + nz) % nz
        pos = jnp.zeros_like(e)
        for p, d in enumerate(order):
            pos = jnp.where(dz == d, p, pos)
        return ((pos * nyc + e % nyc) * cap).astype(F32)

    with jax.named_scope("slots"):
        ti = lax.broadcasted_iota(jnp.int32, (tokens, tokens), 0)
        tj = lax.broadcasted_iota(jnp.int32, (tokens, tokens), 1)
        er = lax.broadcasted_iota(jnp.int32, (64, tokens), 0)
        e0r, e1r = ids_t[0:1, :], ids_t[1:2, :]
        hit0, hit1 = er == e0r, er == e1r
        mbr = jnp.where(hit0 | hit1, 1.0, 0.0).astype(BF16)
        before = jnp.where(ti < tj, 1.0, 0.0).astype(BF16)
        earlier_r = jnp.dot(mbr, before, preferred_element_type=F32)
        slot0r = place(e0r) + jnp.sum(jnp.where(hit0, earlier_r, 0.0), axis=0, keepdims=True)
        slot1r = place(e1r) + jnp.sum(jnp.where(hit1, earlier_r, 0.0), axis=0, keepdims=True)

    def pick_rows(start, count):
        at = (lax.broadcasted_iota(jnp.int32, (count, tokens), 0) + start).astype(F32)
        return jnp.where((at == slot0r) | (at == slot1r), 1.0, 0.0).astype(BF16)

    def fill(p):
        pick = pick_rows(p * group, group)
        if whole[p]:
            at = pl.ds(whole_at[p] * group, group)
            for q in range(4):
                send_full[q, at, :] = jnp.dot(
                    pick, normed[q], preferred_element_type=F32
                ).astype(BF16)
        else:
            at = pl.ds(part_at[p] * group, group)
            send_part[at, :] = jnp.dot(pick, normed[x], preferred_element_type=F32).astype(BF16)

    def send_rows(p):
        dz = order[p]
        k = p // per_chunk
        to_z = (z + dz) % nz

        def send(j, c):
            other = (yc + j) % nyc
            there = pl.ds(pl.multiple_of((p * nyc + yc) * cap, cap), cap)
            if whole[p]:
                here = pl.ds(pl.multiple_of((whole_at[p] * nyc + other) * cap, cap), cap)
                copy = rdma(
                    send_full.at[:, here, :],
                    xin.at[:, there, :],
                    A2A_S, A2A_R, k, to_z * nyc + other, x,
                )
            else:
                here = pl.ds(pl.multiple_of((part_at[p] * nyc + other) * cap, cap), cap)
                copy = rdma(
                    send_part.at[here, :],
                    xin.at[x, there, :],
                    A2P_S, A2P_R, k, to_z * nyc + other, x,
                )
            copy.start()
            return c

        lax.fori_loop(1 if dz == 0 else 0, nyc, send, 0)

    def send_chunk(k):
        for p in range(k * per_chunk, (k + 1) * per_chunk):
            fill(p)
        for p in range(k * per_chunk, (k + 1) * per_chunk):
            send_rows(p)

    mine = pl.ds(pl.multiple_of((own * nyc + yc) * cap, cap), cap)

    def keep_own():
        if whole[own]:
            here = pl.ds(pl.multiple_of((whole_at[own] * nyc + yc) * cap, cap), cap)
            for q in range(4):
                xin[q, mine, :] = send_full[q, here, :]
        else:
            here = pl.ds(pl.multiple_of((part_at[own] * nyc + yc) * cap, cap), cap)
            xin[x, mine, :] = send_part[here, :]

    def at_chunk(k):
        return pl.ds(k * rows, rows)

    def parts_of(k):
        n = sum(whole[k * per_chunk : (k + 1) * per_chunk]) * group
        return k * rows, n, k * rows + n, rows - n

    def less_own(k, is_whole):
        return cap if own // per_chunk == k and bool(whole[own]) == is_whole else 0

    def wait_in(k):
        w0, wn, g0, gn = parts_of(k)
        if wn:
            region = xin.at[:, pl.ds(w0, wn - less_own(k, True)), :]
            rdma(region, region, A2A_S, A2A_R, k, ep, xp).wait_recv()
        if gn:
            region = xin.at[x, pl.ds(g0, gn - less_own(k, False)), :]
            rdma(region, region, A2P_S, A2P_R, k, ep, xp).wait_recv()

    def gather_start(k):
        _, _, g0, gn = parts_of(k)
        if gn:
            region = xin.at[x, pl.ds(g0, gn), :]
            rdma(region, region, AGR_S, AGR_R, k, ep, xp).start()
            rdma(region, region, AGL_S, AGL_R, k, ep, xm).start()

    def gather_forward(k):
        _, _, g0, gn = parts_of(k)
        if gn:
            left = xin.at[xm, pl.ds(g0, gn), :]
            rdma(left, left, AGR_S, AGR_R, k, ep, xp).wait_recv()
            top = xin.at[xm, pl.ds(g0, gn // 2), :]
            rdma(top, top, FWR_S, FWR_R, k, ep, xp).start()
            right = xin.at[xp, pl.ds(g0, gn), :]
            rdma(right, right, AGL_S, AGL_R, k, ep, xm).wait_recv()
            low = xin.at[xp, pl.ds(g0 + gn // 2, gn // 2), :]
            rdma(low, low, FWL_S, FWL_R, k, ep, xm).start()

    def gather_done(k):
        _, _, g0, gn = parts_of(k)
        if gn:
            top = xin.at[xo, pl.ds(g0, gn // 2), :]
            low = xin.at[xo, pl.ds(g0 + gn // 2, gn // 2), :]
            rdma(top, top, FWR_S, FWR_R, k, ep, xp).wait_recv()
            rdma(low, low, FWL_S, FWL_R, k, ep, xm).wait_recv()

    hidden_dev = wg.shape[1]
    nb = min(256, hidden_dev)

    def compute(k):
        def up(n, c):
            cols = pl.ds(pl.multiple_of(n * nb, nb), nb)
            g = jnp.zeros((rows, nb), F32)
            u = jnp.zeros((rows, nb), F32)
            for q in range(4):
                xq = xin[q, at_chunk(k), :]
                ws = pl.ds(q * quarter, quarter)
                g = g + jnp.dot(xq, wg[ws, cols], preferred_element_type=F32)
                u = u + jnp.dot(xq, wu[ws, cols], preferred_element_type=F32)
            hid[:, cols] = (g / (1.0 + jnp.exp(-g)) * u).astype(BF16)
            return c

        lax.fori_loop(0, hidden_dev // nb, up, 0)

        def down(d):
            cols = pl.ds(pl.multiple_of(d * quarter, quarter), quarter)
            part[k, d] = jnp.dot(
                hid[...], wd[:, cols], preferred_element_type=F32
            ).astype(BF16)

        down(xo)
        down(xp)
        rdma(
            part.at[k, xo, pl.ds(0, half), :], s1r.at[k], S1R_S, S1R_R, k, ep, xp
        ).start()
        rdma(
            part.at[k, xo, pl.ds(half, half), :], s1l.at[k], S1L_S, S1L_R, k, ep, xm
        ).start()
        down(xm)
        down(x)

    def scatter_add(k):
        rdma(s1r.at[k], s1r.at[k], S1R_S, S1R_R, k, ep, xp).wait_recv()
        top = pl.ds(0, half)
        part[k, xp, top, :] = (
            part[k, xp, top, :].astype(F32) + s1r[k].astype(F32)
        ).astype(BF16)
        rdma(s1l.at[k], s1l.at[k], S1L_S, S1L_R, k, ep, xm).wait_recv()
        low = pl.ds(half, half)
        part[k, xm, low, :] = (
            part[k, xm, low, :].astype(F32) + s1l[k].astype(F32)
        ).astype(BF16)
        rdma(part.at[k, xp], s2r.at[k], S2R_S, S2R_R, k, ep, xp).start()
        rdma(part.at[k, xm], s2l.at[k], S2L_S, S2L_R, k, ep, xm).start()

    def give_back(k):
        rdma(s2r.at[k], s2r.at[k], S2R_S, S2R_R, k, ep, xp).wait_recv()
        rdma(s2l.at[k], s2l.at[k], S2L_S, S2L_R, k, ep, xm).wait_recv()
        sums = part[k, x].astype(F32) + s2r[k].astype(F32) + s2l[k].astype(F32)
        ans[at_chunk(k), :] = sums.astype(BF16)
        if k == own // per_chunk:
            ret[mine, :] = ans[mine, :]
        for p in range(k * per_chunk, (k + 1) * per_chunk):
            dz = order[p]
            to_z = (z - dz + nz) % nz

            def send(j, c, p=p, to_z=to_z):
                other = (yc + j) % nyc
                here = pl.ds(pl.multiple_of((p * nyc + other) * cap, cap), cap)
                there = pl.ds(pl.multiple_of((p * nyc + yc) * cap, cap), cap)
                rdma(
                    ans.at[here, :], ret.at[there, :], RET_S, RET_R, k,
                    to_z * nyc + other, x,
                ).start()
                return c

            lax.fori_loop(1 if dz == 0 else 0, nyc, send, 0)

    length, channels_dev = value.shape
    lane_groups = channels_dev // 128
    reach = taps.shape[0]
    m_rows = length // 4
    core = ep % 2
    partner = ep + 1 - 2 * core
    w_half = channels_dev // 2
    w_mine = pl.ds(pl.multiple_of(core * w_half, w_half), w_half)
    w_theirs = pl.ds(pl.multiple_of((1 - core) * w_half, w_half), w_half)
    w_top = pl.ds(pl.multiple_of(core * w_half, w_half // 2), w_half // 2)
    w_low = pl.ds(pl.multiple_of(core * w_half + w_half // 2, w_half // 2), w_half // 2)

    def mcopy(src, dst, row, to_ep, to_x):
        return pltpu.make_async_remote_copy(
            src_ref=src,
            dst_ref=dst,
            send_sem=msend.at[row],
            recv_sem=mrecv.at[row],
            device_id=(to_ep, to_x),
            device_id_type=MESH,
        )

    def mixer_gate():
        loads[1].wait()
        loads[2].wait()

        def rows_of(i, c):
            at = pl.ds(pl.multiple_of(i * 32, 32), 32)
            v = value[at, :].astype(F32)
            g = gate[at, :].astype(F32)
            y = (v * (1.0 / (1.0 + jnp.exp(-g)))).astype(BF16)
            wide = y.astype(F32)
            to = pl.ds(pl.multiple_of(i * 32 + 32, 32), 32)
            for h in range(lane_groups):
                gated[h, to, :] = wide[:, h * 128 : (h + 1) * 128]
            tail[...] = y
            return c

        lax.fori_loop(0, length // 32, rows_of, 0)

    def halo_send():
        mcopy(tail, halo, HALO, (ep + 1) % n_ep, x).start()

    def mixer_conv():
        mcopy(tail, halo, HALO, (ep + 1) % n_ep, x).wait_recv()
        before_first = jnp.where(ep == 0, 0.0, halo[...].astype(F32))
        for h in range(lane_groups):
            gated[h, 0:32, :] = before_first[:, h * 128 : (h + 1) * 128]
        cb = 64
        for h in range(lane_groups):
            lanes = slice(h * 128, (h + 1) * 128)

            def rows_of(i, c, h=h, lanes=lanes):
                base = pl.multiple_of(i * cb, cb)
                window = gated.at[h, pl.ds(base, cb + 32), :]
                acc = jnp.zeros((cb, 128), F32)
                for j in range(reach):
                    acc = acc + taps[j : j + 1, lanes] * window[32 - j : 32 - j + cb, :]
                conv[pl.ds(base, cb), lanes] = acc
                return c

            lax.fori_loop(0, length // cb, rows_of, 0)

        sb = 128
        lane = lax.broadcasted_iota(jnp.int32, (sb, 128), 1)
        for i in range(length // sb):
            c = conv[i * sb : (i + 1) * sb, :]
            total = jnp.sum(c, axis=1, keepdims=True)
            squares = jnp.sum(c * c, axis=1, keepdims=True)
            both = jnp.where(lane == 0, total, jnp.where(lane == 1, squares, 0.0))
            stat[:, i * sb : (i + 1) * sb] = both.T[0:8, :]
        for n, (row, to_x) in enumerate(((STAT_P, xp), (STAT_M, xm), (STAT_O, xo))):
            mcopy(stat, stat_in.at[n], row, ep, to_x).start()

    def mixer_out():
        for n, row in enumerate((STAT_P, STAT_M, STAT_O)):
            mcopy(stat, stat_in.at[n], row, ep, xp).wait_recv()
        sums = stat[...] + stat_in[0] + stat_in[1] + stat_in[2]
        channels = channels_dev * 4
        sb = 128
        for i in range(length // sb):
            at = slice(i * sb, (i + 1) * sb)
            mean = sums[0:1, at] / channels
            variance = sums[1:2, at] / channels - mean * mean
            scale = lax.rsqrt(variance + eps_norm)
            r = lax.broadcasted_iota(jnp.int32, (128, sb), 0)
            cols = jnp.where(r == 0, mean, jnp.where(r == 1, scale, 0.0)).T
            v = (conv[at, :] - cols[:, 0:1]) * cols[:, 1:2] * ln_gain[...]
            act[at, :] = (v / (1.0 + jnp.exp(-v))).astype(BF16)
        for row, to_x in ((ACT_P, xp), (ACT_M, xm), (ACT_O, xo)):
            at = pl.ds(pl.multiple_of(to_x * m_rows, m_rows), m_rows)
            mcopy(act.at[at, :], act_in.at[x], row, ep, to_x).start()
        act_in[x] = act[pl.ds(pl.multiple_of(x * m_rows, m_rows), m_rows), :]

    def w_start():
        loads[3].wait()
        mcopy(w_out.at[x, w_mine, :], w_out.at[x, w_mine, :], WR, ep, xp).start()
        mcopy(w_out.at[x, w_mine, :], w_out.at[x, w_mine, :], WL, ep, xm).start()

    def w_forward():
        left = w_out.at[xm, w_mine, :]
        mcopy(left, left, WR, ep, xp).wait_recv()
        top = w_out.at[xm, w_top, :]
        mcopy(top, top, WFR, ep, xp).start()
        mcopy(left, left, WC_M, partner, x).start()
        right = w_out.at[xp, w_mine, :]
        mcopy(right, right, WL, ep, xm).wait_recv()
        low = w_out.at[xp, w_low, :]
        mcopy(low, low, WFL, ep, xm).start()
        mcopy(right, right, WC_P, partner, x).start()

    def w_share():
        top = w_out.at[xo, w_top, :]
        low = w_out.at[xo, w_low, :]
        mcopy(top, top, WFR, ep, xp).wait_recv()
        mcopy(low, low, WFL, ep, xm).wait_recv()
        opposite = w_out.at[xo, w_mine, :]
        mcopy(opposite, opposite, WC_O, partner, x).start()

    def mixer_project():
        for row, q in ((ACT_P, xm), (ACT_M, xp), (ACT_O, xo)):
            mcopy(act_in.at[q], act_in.at[q], row, ep, xp).wait_recv()
        for row, q in ((WC_M, xm), (WC_P, xp), (WC_O, xo)):
            theirs = w_out.at[q, w_theirs, :]
            mcopy(theirs, theirs, row, partner, x).wait_recv()

        def project(n, c):
            cols = pl.ds(pl.multiple_of(n * 256, 256), 256)
            sums = jnp.zeros((m_rows, 256), F32)
            for q in range(4):
                sums = sums + jnp.dot(act_in[q], w_out[q, :, cols], preferred_element_type=F32)
            mixed[:, cols] = sums.astype(BF16)
            return c

        lax.fori_loop(0, width // 256, project, 0)

    def combine(k):
        region = ret.at[pl.ds(k * rows, rows - less_own(k, bool(whole[own]))), :]
        rdma(region, region, RET_S, RET_R, k, ep, xp).wait_recv()
        slot0c, slot1c = columns[:, 0:1], columns[:, 1:2]
        at = (lax.broadcasted_iota(jnp.int32, (tokens, rows), 1) + k * rows).astype(F32)
        w = jnp.where(at == slot0c, columns[:, 2:3], 0.0)
        w = w + jnp.where(at == slot1c, columns[:, 3:4], 0.0)
        high = w.astype(BF16)
        low = (w - high.astype(F32)).astype(BF16)
        got = ret[at_chunk(k), :]
        sums = jnp.dot(high, got, preferred_element_type=F32)
        sums = sums + jnp.dot(low, got, preferred_element_type=F32)
        total[...] = sums if k == 0 else total[...] + sums

    def run(step, *k):
        with jax.named_scope(step.__name__ + "".join(f"#{i}" for i in k)):
            step(*k)

    run(mixer_gate)
    with jax.named_scope("barrier_wait"):
        pl.semaphore_wait(barrier, n_ep - 1 + 3)
    halo_send()
    run(w_start)
    with jax.named_scope("norm"):
        loads[0].wait()
        lax.fori_loop(0, tokens // block, norm_rows, 0)
    for k in range(n_chunks):
        run(send_chunk, k)
    keep_own()
    turn = lax.broadcasted_iota(jnp.int32, (128, tokens), 0)
    table = jnp.where(turn == 0, slot0r, jnp.where(turn == 1, slot1r, 0.0))
    table = jnp.where(turn == 2, route_t[0:1, :], table)
    table = jnp.where(turn == 3, route_t[1:2, :], table)
    columns = table.T

    def compute_after(k):
        run(wait_in, k)
        run(gather_done, k)
        run(compute, k)

    run(mixer_conv)
    run(wait_in, 0)
    run(gather_start, 0)
    run(mixer_out)
    run(w_forward)
    run(gather_forward, 0)
    for load in loads[4:]:
        load.wait()
    run(gather_done, 0)
    run(compute, 0)
    run(w_share)
    run(wait_in, 1)
    run(gather_start, 1)
    run(scatter_add, 0)
    run(gather_forward, 1)
    run(mixer_project)
    run(give_back, 0)
    run(gather_done, 1)
    run(compute, 1)
    run(wait_in, 2)
    run(gather_start, 2)
    run(gather_forward, 2)
    run(gather_done, 2)
    run(compute, 2)
    run(scatter_add, 1)
    run(wait_in, 3)
    run(compute, 3)
    run(scatter_add, 2)
    run(give_back, 1)
    run(combine, 0)
    run(scatter_add, 3)
    run(give_back, 2)
    run(combine, 1)
    run(give_back, 3)
    run(combine, 2)
    run(combine, 3)
    out[...] = total[...].astype(BF16)

    for k in range(n_chunks):
        w0, wn, g0, gn = parts_of(k)
        if wn:
            region = send_full.at[:, pl.ds(0, wn - less_own(k, True)), :]
            rdma(region, region, A2A_S, A2A_R, k, ep, xp).wait_send()
        if gn:
            region = send_part.at[pl.ds(0, gn - less_own(k, False)), :]
            rdma(region, region, A2P_S, A2P_R, k, ep, xp).wait_send()
            region = xin.at[x, pl.ds(g0, gn), :]
            rdma(region, region, AGR_S, AGR_R, k, ep, xp).wait_send()
            rdma(region, region, AGL_S, AGL_R, k, ep, xm).wait_send()
            region = xin.at[x, pl.ds(g0, gn // 2), :]
            rdma(region, region, FWR_S, FWR_R, k, ep, xp).wait_send()
            rdma(region, region, FWL_S, FWL_R, k, ep, xm).wait_send()
        back = ans.at[pl.ds(k * rows, rows - less_own(k, bool(whole[own]))), :]
        rdma(s1r.at[k], s1r.at[k], S1R_S, S1R_R, k, ep, xp).wait_send()
        rdma(s1l.at[k], s1l.at[k], S1L_S, S1L_R, k, ep, xm).wait_send()
        rdma(s2r.at[k], s2r.at[k], S2R_S, S2R_R, k, ep, xp).wait_send()
        rdma(s2l.at[k], s2l.at[k], S2L_S, S2L_R, k, ep, xm).wait_send()
        rdma(back, back, RET_S, RET_R, k, ep, xp).wait_send()
    mcopy(tail, tail, HALO, ep, xp).wait_send()
    for row in (STAT_P, STAT_M, STAT_O):
        mcopy(stat, stat, row, ep, xp).wait_send()
    for row in (ACT_P, ACT_M, ACT_O):
        mcopy(act_in.at[0], act_in.at[0], row, ep, xp).wait_send()
    for row in (WR, WL, WC_P, WC_M, WC_O):
        sent = w_out.at[x, w_mine, :]
        mcopy(sent, sent, row, ep, xp).wait_send()
    for row in (WFR, WFL):
        sent = w_out.at[x, w_top, :]
        mcopy(sent, sent, row, ep, xp).wait_send()


def on_device(
    glu_value,
    glu_gate,
    conv_kernel,
    ln_gain,
    out_weight,
    moe_input,
    moe_gain,
    gate_weight,
    up_weight,
    down_weight,
    expert_ids,
    route_weight,
):
    tokens, width = moe_input.shape
    length, channels_dev = glu_value.shape
    ep_count = lax.axis_size("ep")
    nyc, order, whole, per_chunk = layout_of(ep_count)
    nz = ep_count // nyc
    cap = 16
    hidden_dev = gate_weight.shape[2]
    quarter = width // 4
    n_chunks = nz // per_chunk
    rows = per_chunk * nyc * cap
    slots = ep_count * cap
    vmem = pl.BlockSpec(memory_space=pltpu.VMEM)
    hbm = pl.BlockSpec(memory_space=pl.ANY)
    n_whole = sum(whole) * nyc * cap
    cfg = (nz, nyc, order, whole, per_chunk, cap)
    return pl.pallas_call(
        functools.partial(block_kernel, cfg),
        out_shape=(
            jax.ShapeDtypeStruct((length // 4, width), BF16),
            jax.ShapeDtypeStruct((tokens, quarter), BF16),
        ),
        in_specs=[vmem] * 5 + [hbm] * 7,
        out_specs=(vmem, vmem),
        scratch_shapes=[
            pltpu.VMEM((tokens, width), BF16),
            pltpu.VMEM((length, channels_dev), BF16),
            pltpu.VMEM((length, channels_dev), BF16),
            pltpu.VMEM((4, channels_dev, width), BF16),
            pltpu.VMEM((width, hidden_dev), BF16),
            pltpu.VMEM((width, hidden_dev), BF16),
            pltpu.VMEM((hidden_dev, width), BF16),
            pltpu.VMEM((4, tokens, quarter), BF16),
            pltpu.VMEM((4, max(n_whole, 16), quarter), BF16),
            pltpu.VMEM((max(slots - n_whole, 16), quarter), BF16),
            pltpu.VMEM((4, slots, quarter), BF16),
            pltpu.VMEM((rows, hidden_dev), BF16),
            pltpu.VMEM((n_chunks, 4, rows, quarter), BF16),
            pltpu.VMEM((n_chunks, rows // 2, quarter), BF16),
            pltpu.VMEM((n_chunks, rows // 2, quarter), BF16),
            pltpu.VMEM((n_chunks, rows, quarter), BF16),
            pltpu.VMEM((n_chunks, rows, quarter), BF16),
            pltpu.VMEM((slots, quarter), BF16),
            pltpu.VMEM((slots, quarter), BF16),
            pltpu.VMEM((32, channels_dev), BF16),
            pltpu.VMEM((32, channels_dev), BF16),
            pltpu.VMEM((channels_dev // 128, length + 32, 128), F32),
            pltpu.VMEM((length, channels_dev), F32),
            pltpu.VMEM((8, length), F32),
            pltpu.VMEM((3, 8, length), F32),
            pltpu.VMEM((length, channels_dev), BF16),
            pltpu.VMEM((4, length // 4, channels_dev), BF16),
            pltpu.VMEM((tokens, quarter), F32),
            pltpu.SemaphoreType.DMA((7,)),
            pltpu.SemaphoreType.DMA((22, n_chunks)),
            pltpu.SemaphoreType.DMA((14,)),
            pltpu.SemaphoreType.DMA((14,)),
        ],
        compiler_params=pltpu.CompilerParams(
            collective_id=0, has_side_effects=True, vmem_limit_bytes=60 * 1024 * 1024
        ),
        name="block",
    )(
        moe_gain[None, :],
        expert_ids.T,
        route_weight.T,
        conv_kernel,
        ln_gain[None, :],
        moe_input,
        glu_value,
        glu_gate,
        out_weight,
        gate_weight,
        up_weight,
        down_weight,
    )


def solution(mesh):
    in_specs = (
        P("ep", "tp"),
        P("ep", "tp"),
        P(None, "tp"),
        P("tp"),
        P("tp", None),
        P("ep", None),
        P(),
        P("ep", None, "tp"),
        P("ep", None, "tp"),
        P("ep", "tp", None),
        P("ep", None),
        P("ep", None),
    )
    out_specs = (P(("ep", "tp"), None), P("ep", "tp"))
    return jax.shard_map(
        on_device, mesh=mesh, in_specs=in_specs, out_specs=out_specs, check_vma=False
    )
```

time: 154 us -> 112 us (0.73); the launches traced: 152 us -> 112 us
  between operations: 14.1 us -> 0.64 us
  blocking collectives: 8.77 us -> 0 us
  Pallas kernels: 114 us -> 108 us
  starting transfers between devices: 4.62 us -> 0 us
  other arithmetic: 3.71 us -> 0 us
  matrix products: 2.14 us -> 0 us
  local copies, waits for them, and re-layouts: 5.3 us -> 3.55 us
    psum x1 -> x0, blocking collectives: 8.77 us -> none  [on_device(): lax.psum((jnp.sum(convolved, axis=1), jnp.sum(convolved * convolved, axis...]
    pallas_call x1, Pallas kernels: 114 us -> 108 us  [on_device(): pl.pallas_call(functools.partial(block_kernel, cfg), out_shape=(jax.Shape...]
    ppermute x1 -> x0, starting transfers between devices: 4.58 us -> none  [from_behind(): return lax.ppermute(value, axis, pairs)]
    reduce_sum x1 -> x0, other arithmetic: 2.38 us -> none  [on_device(): jnp.sum(convolved, axis=1)]
    dot_general x1 -> x0, matrix products: 2.14 us -> none  [on_device(): jnp.dot(activated, out_weight, preferred_element_type=F32).astype(BF16)]
    slice x3 -> x0, local copies, waits for them, and re-layouts: 2.01 us -> none  [the longest x2 2 us: on_device(): conv_kernel[tap_index] * padded[begin:begin + length]]
    unnamed x11 -> x2, local copies, waits for them, and re-layouts: 3.29 us -> 3.55 us
  transfers between devices with their start and end apart: 2 -> 0, of which waited for: 0 -> 0; matrix products, arithmetic and copies ran while one was open for 2% -> 0% of each run, Pallas kernels for 75% -> 0%
where the time goes in v2:
time: 112 us
  Pallas kernels  108 us (96%)
  local copies, waits for them, and re-layouts  3.55 us (3%)
    pallas_call x1, Pallas kernels, on_device(): pl.pallas_call(functools.partial(block_kernel, cfg), out_shape=(jax.Shape...  108 us
    unnamed x2, local copies, waits for them, and re-layouts  3.55 us

profile of v2, /device:TPU:1, one launch (start us, length us, event | category | flops | bytes accessed | tf_op | source)
XLA Modules:
  0.0 112.0 jit_solution(4646861658620034638)
XLA Ops:
  0.6 107.9 %block.1 = (bf16[128,2048]{1,0:T(8,128)(2,1)}, bf16[256,512]{1,0:T(8,128)(2,1)}) custom-call(f32[1,2048]{1,0:T(1,128)} %bitcast.4, s32[2,256]{1,0:T(2,128)} %bitcast.5, f32[2,256]{1,0:T(2,128)} %bitcast.6, f32[31,256]{1,0:T(8,128)} %taps.1, f32[1,256]{1,0:T(1,128)} %bitcast.7, bf16[256,2048]{1,0:T(8,128)(2,1)} %moe_hbm.1, bf16[512,256]{1,0:T(8,128)(2,1)} %value_hbm.1, ...), custom_call_target="tpu_custom_call" | custom-call | tf_op jit(solution)/shard_map/block/pallas_call | solution.py:617
  108.5 1.9 %copy.16 = bf16[128,2048]{1,0:T(8,128)(2,1)} copy(bf16[128,2048]{1,0:T(8,128)(2,1)} %get-tuple-element.4) | data formatting | bytes 1048576
  110.4 1.7 %copy.17 = bf16[256,512]{1,0:T(8,128)(2,1)} copy(bf16[256,512]{1,0:T(8,128)(2,1)} %get-tuple-element.5) | data formatting | bytes 524288

commit v3 on v2

--- a/solution.py
+++ b/solution.py
@@ -16,22 +16,29 @@
 A2A_S, A2A_R, AGR_S, AGR_R, AGL_S, AGL_R, FWR_S, FWR_R, FWL_S, FWL_R = range(10)
 S1R_S, S1R_R, S1L_S, S1L_R, S2R_S, S2R_R, S2L_S, S2L_R, RET_S, RET_R = range(10, 20)
 A2P_S, A2P_R = 20, 21
-HALO, STAT_P, STAT_M, STAT_O, ACT_P, ACT_M, ACT_O, WR, WL, WFR, WFL, WC_P, WC_M, WC_O = range(14)
+HALO, STAT_P, STAT_M, STAT_O, ACT_P, ACT_M, ACT_O, WR, WL, WFR, WFL, YR, YL, YFR, YFL, WC = range(16)
+
+
+NARROW = False
 
 
 def layout_of(ep_count):
     if ep_count == 64:
-        return 8, (5, 3, 6, 4, 7, 2, 0, 1), (0, 0, 0, 0, 1, 1, 1, 1), 2
-    return 2, (2, 3, 1, 0), (0, 0, 1, 1), 1
+        return 8, (0, 7, 2, 5, 3, 4, 1, 6), (0, 0, 0, 0, 0, 0, 1, 1), 2
+    if ep_count == 32:
+        return 8, (2, 0, 3, 1), (0, 1, 0, 1), 1
+    if ep_count == 8 and NARROW:
+        return 8, (0,), (0,), 1
+    return 2, (2, 0, 3, 1), (0, 1, 0, 1), 1
 
 
 def block_kernel(
     cfg,
-    gain,
-    ids_t,
-    route_t,
-    taps,
-    ln_gain,
+    gain_hbm,
+    ids_hbm,
+    route_hbm,
+    taps_hbm,
+    ln_gain_hbm,
     moe_hbm,
     value_hbm,
     gate_hbm,
@@ -41,6 +48,11 @@
     w_down_hbm,
     mixed,
     out,
+    gain,
+    ids_t,
+    route_t,
+    taps,
+    ln_gain,
     moe_in,
     value,
     gate,
@@ -114,11 +126,16 @@
                 (w_gate_hbm.at[0], wg),
                 (w_up_hbm.at[0], wu),
                 (w_down_hbm.at[0], wd),
+                (ids_hbm, ids_t),
+                (gain_hbm, gain),
+                (route_hbm, route_t),
+                (taps_hbm, taps),
+                (ln_gain_hbm, ln_gain),
             )
         )
     ]
-    for load in loads:
-        load.start()
+    for i in (7, 0, 8, 1, 2, 3, 9, 10, 11, 4, 5, 6):
+        loads[i].start()
 
     def rdma(src, dst, row_s, row_r, k, to_ep, to_x):
         return pltpu.make_async_remote_copy(
@@ -149,6 +166,7 @@
         return ((pos * nyc + e % nyc) * cap).astype(F32)
 
     with jax.named_scope("slots"):
+        loads[7].wait()
         ti = lax.broadcasted_iota(jnp.int32, (tokens, tokens), 0)
         tj = lax.broadcasted_iota(jnp.int32, (tokens, tokens), 1)
         er = lax.broadcasted_iota(jnp.int32, (64, tokens), 0)
@@ -203,9 +221,11 @@
 
         lax.fori_loop(1 if dz == 0 else 0, nyc, send, 0)
 
-    def send_chunk(k):
+    def fill_chunk(k):
         for p in range(k * per_chunk, (k + 1) * per_chunk):
             fill(p)
+
+    def send_chunk(k):
         for p in range(k * per_chunk, (k + 1) * per_chunk):
             send_rows(p)
 
@@ -344,11 +364,12 @@
     m_rows = length // 4
     core = ep % 2
     partner = ep + 1 - 2 * core
-    w_half = channels_dev // 2
-    w_mine = pl.ds(pl.multiple_of(core * w_half, w_half), w_half)
-    w_theirs = pl.ds(pl.multiple_of((1 - core) * w_half, w_half), w_half)
-    w_top = pl.ds(pl.multiple_of(core * w_half, w_half // 2), w_half // 2)
-    w_low = pl.ds(pl.multiple_of(core * w_half + w_half // 2, w_half // 2), w_half // 2)
+    ny = nyc // 2
+    yy = yc // 2
+    y_up = z * nyc + (yy + 1) % ny * 2 + core
+    y_down = z * nyc + (yy + ny - 1) % ny * 2 + core
+    w_rows = channels_dev // nyc
+    others = (xm, xp, xo)
 
     def mcopy(src, dst, row, to_ep, to_x):
         return pltpu.make_async_remote_copy(
@@ -434,41 +455,68 @@
 
     def w_start():
         loads[3].wait()
-        mcopy(w_out.at[x, w_mine, :], w_out.at[x, w_mine, :], WR, ep, xp).start()
-        mcopy(w_out.at[x, w_mine, :], w_out.at[x, w_mine, :], WL, ep, xm).start()
+        sent = w_out.at[x, yy, core]
+        mcopy(sent, sent, WR, ep, xp).start()
+        mcopy(sent, sent, WL, ep, xm).start()
+
+    def along_y(q):
+        if ny > 1:
+            sent = w_out.at[q, yy, core]
+            mcopy(sent, sent, YR, y_up, x).start()
+            mcopy(sent, sent, YL, y_down, x).start()
 
     def w_forward():
-        left = w_out.at[xm, w_mine, :]
+        left = w_out.at[xm, yy, core]
         mcopy(left, left, WR, ep, xp).wait_recv()
-        top = w_out.at[xm, w_top, :]
+        top = w_out.at[xm, yy, core, pl.ds(0, w_rows // 2), :]
         mcopy(top, top, WFR, ep, xp).start()
-        mcopy(left, left, WC_M, partner, x).start()
-        right = w_out.at[xp, w_mine, :]
+        right = w_out.at[xp, yy, core]
         mcopy(right, right, WL, ep, xm).wait_recv()
-        low = w_out.at[xp, w_low, :]
+        low = w_out.at[xp, yy, core, pl.ds(w_rows // 2, w_rows // 2), :]
         mcopy(low, low, WFL, ep, xm).start()
-        mcopy(right, right, WC_P, partner, x).start()
-
-    def w_share():
-        top = w_out.at[xo, w_top, :]
-        low = w_out.at[xo, w_low, :]
+        along_y(xm)
+        along_y(xp)
+
+    def w_along_y():
+        top = w_out.at[xo, yy, core, pl.ds(0, w_rows // 2), :]
+        low = w_out.at[xo, yy, core, pl.ds(w_rows // 2, w_rows // 2), :]
         mcopy(top, top, WFR, ep, xp).wait_recv()
         mcopy(low, low, WFL, ep, xm).wait_recv()
-        opposite = w_out.at[xo, w_mine, :]
-        mcopy(opposite, opposite, WC_O, partner, x).start()
+        along_y(xo)
+
+    def w_forward_y():
+        if ny > 1:
+            three = w_out.at[pl.ds(0, 3), yy, core]
+            mcopy(three, three, YR, y_up, x).wait_recv()
+            for q in others:
+                top = w_out.at[q, (yy + ny - 1) % ny, core, pl.ds(0, w_rows // 2), :]
+                mcopy(top, top, YFR, y_up, x).start()
+            mcopy(three, three, YL, y_down, x).wait_recv()
+            for q in others:
+                low = w_out.at[q, (yy + 1) % ny, core, pl.ds(w_rows // 2, w_rows // 2), :]
+                mcopy(low, low, YFL, y_down, x).start()
+
+    def w_share():
+        if ny > 1:
+            three = w_out.at[pl.ds(0, 3), yy, core, pl.ds(0, w_rows // 2), :]
+            mcopy(three, three, YFR, y_up, x).wait_recv()
+            mcopy(three, three, YFL, y_down, x).wait_recv()
+        for q in others:
+            sent = w_out.at[q, :, core]
+            mcopy(sent, sent, WC, partner, x).start()
 
     def mixer_project():
         for row, q in ((ACT_P, xm), (ACT_M, xp), (ACT_O, xo)):
             mcopy(act_in.at[q], act_in.at[q], row, ep, xp).wait_recv()
-        for row, q in ((WC_M, xm), (WC_P, xp), (WC_O, xo)):
-            theirs = w_out.at[q, w_theirs, :]
-            mcopy(theirs, theirs, row, partner, x).wait_recv()
+        theirs = w_out.at[pl.ds(0, 3), :, 1 - core]
+        mcopy(theirs, theirs, WC, partner, x).wait_recv()
 
         def project(n, c):
             cols = pl.ds(pl.multiple_of(n * 256, 256), 256)
             sums = jnp.zeros((m_rows, 256), F32)
             for q in range(4):
-                sums = sums + jnp.dot(act_in[q], w_out[q, :, cols], preferred_element_type=F32)
+                w = w_out[q, :, :, :, cols].reshape(channels_dev, 256)
+                sums = sums + jnp.dot(act_in[q], w, preferred_element_type=F32)
             mixed[:, cols] = sums.astype(BF16)
             return c
 
@@ -486,70 +534,79 @@
         got = ret[at_chunk(k), :]
         sums = jnp.dot(high, got, preferred_element_type=F32)
         sums = sums + jnp.dot(low, got, preferred_element_type=F32)
-        total[...] = sums if k == 0 else total[...] + sums
+        total[...] = total[...] + sums
 
     def run(step, *k):
+        if k and k[0] >= n_chunks:
+            return
         with jax.named_scope(step.__name__ + "".join(f"#{i}" for i in k)):
             step(*k)
 
+    with jax.named_scope("norm"):
+        loads[0].wait()
+        loads[8].wait()
+        lax.fori_loop(0, tokens // block, norm_rows, 0)
+    run(fill_chunk, 0)
     run(mixer_gate)
     with jax.named_scope("barrier_wait"):
         pl.semaphore_wait(barrier, n_ep - 1 + 3)
     halo_send()
+    run(send_chunk, 0)
     run(w_start)
-    with jax.named_scope("norm"):
-        loads[0].wait()
-        lax.fori_loop(0, tokens // block, norm_rows, 0)
-    for k in range(n_chunks):
-        run(send_chunk, k)
+    for k in range(1, n_chunks):
+        run(fill_chunk, k)
     keep_own()
+    loads[9].wait()
     turn = lax.broadcasted_iota(jnp.int32, (128, tokens), 0)
     table = jnp.where(turn == 0, slot0r, jnp.where(turn == 1, slot1r, 0.0))
     table = jnp.where(turn == 2, route_t[0:1, :], table)
     table = jnp.where(turn == 3, route_t[1:2, :], table)
     columns = table.T
 
-    def compute_after(k):
-        run(wait_in, k)
-        run(gather_done, k)
-        run(compute, k)
-
+    loads[10].wait()
+    loads[11].wait()
+    total[...] = jnp.zeros_like(total)
+    run(send_chunk, 1)
+    run(send_chunk, 2)
     run(mixer_conv)
+    run(w_forward)
     run(wait_in, 0)
     run(gather_start, 0)
     run(mixer_out)
-    run(w_forward)
+    run(w_along_y)
+    for load in loads[4:7]:
+        load.wait()
     run(gather_forward, 0)
-    for load in loads[4:]:
-        load.wait()
+    run(send_chunk, 3)
+    run(wait_in, 1)
+    run(gather_start, 1)
     run(gather_done, 0)
     run(compute, 0)
-    run(w_share)
-    run(wait_in, 1)
-    run(gather_start, 1)
-    run(scatter_add, 0)
     run(gather_forward, 1)
-    run(mixer_project)
-    run(give_back, 0)
+    run(wait_in, 2)
+    run(gather_start, 2)
     run(gather_done, 1)
     run(compute, 1)
-    run(wait_in, 2)
-    run(gather_start, 2)
     run(gather_forward, 2)
+    run(scatter_add, 1)
+    run(w_forward_y)
     run(gather_done, 2)
     run(compute, 2)
-    run(scatter_add, 1)
     run(wait_in, 3)
     run(compute, 3)
+    run(give_back, 1)
     run(scatter_add, 2)
-    run(give_back, 1)
-    run(combine, 0)
     run(scatter_add, 3)
+    run(w_share)
     run(give_back, 2)
+    run(scatter_add, 0)
+    run(give_back, 3)
     run(combine, 1)
-    run(give_back, 3)
+    run(give_back, 0)
+    run(mixer_project)
     run(combine, 2)
     run(combine, 3)
+    run(combine, 0)
     out[...] = total[...].astype(BF16)
 
     for k in range(n_chunks):
@@ -577,12 +634,21 @@
         mcopy(stat, stat, row, ep, xp).wait_send()
     for row in (ACT_P, ACT_M, ACT_O):
         mcopy(act_in.at[0], act_in.at[0], row, ep, xp).wait_send()
-    for row in (WR, WL, WC_P, WC_M, WC_O):
-        sent = w_out.at[x, w_mine, :]
-        mcopy(sent, sent, row, ep, xp).wait_send()
-    for row in (WFR, WFL):
-        sent = w_out.at[x, w_top, :]
-        mcopy(sent, sent, row, ep, xp).wait_send()
+    sent = w_out.at[x, yy, core]
+    mcopy(sent, sent, WR, ep, xp).wait_send()
+    mcopy(sent, sent, WL, ep, xp).wait_send()
+    sent = w_out.at[x, yy, core, pl.ds(0, w_rows // 2), :]
+    mcopy(sent, sent, WFR, ep, xp).wait_send()
+    mcopy(sent, sent, WFL, ep, xp).wait_send()
+    if ny > 1:
+        sent = w_out.at[pl.ds(0, 3), yy, core]
+        mcopy(sent, sent, YR, y_up, x).wait_send()
+        mcopy(sent, sent, YL, y_down, x).wait_send()
+        sent = w_out.at[pl.ds(0, 3), yy, core, pl.ds(0, w_rows // 2), :]
+        mcopy(sent, sent, YFR, y_up, x).wait_send()
+        mcopy(sent, sent, YFL, y_down, x).wait_send()
+    sent = w_out.at[pl.ds(0, 3), :, core]
+    mcopy(sent, sent, WC, partner, x).wait_send()
 
 
 def on_device(
@@ -617,16 +683,21 @@
     return pl.pallas_call(
         functools.partial(block_kernel, cfg),
         out_shape=(
-            jax.ShapeDtypeStruct((length // 4, width), BF16),
-            jax.ShapeDtypeStruct((tokens, quarter), BF16),
+            pltpu.VMEM((length // 4, width), BF16),
+            pltpu.VMEM((tokens, quarter), BF16),
         ),
-        in_specs=[vmem] * 5 + [hbm] * 7,
+        in_specs=[hbm] * 12,
         out_specs=(vmem, vmem),
         scratch_shapes=[
+            pltpu.VMEM((1, width), F32),
+            pltpu.VMEM(expert_ids.shape[::-1], jnp.int32),
+            pltpu.VMEM(route_weight.shape[::-1], F32),
+            pltpu.VMEM(conv_kernel.shape, F32),
+            pltpu.VMEM((1, channels_dev), F32),
             pltpu.VMEM((tokens, width), BF16),
             pltpu.VMEM((length, channels_dev), BF16),
             pltpu.VMEM((length, channels_dev), BF16),
-            pltpu.VMEM((4, channels_dev, width), BF16),
+            pltpu.VMEM((4, nyc // 2, 2, channels_dev // nyc, width), BF16),
             pltpu.VMEM((width, hidden_dev), BF16),
             pltpu.VMEM((width, hidden_dev), BF16),
             pltpu.VMEM((hidden_dev, width), BF16),
@@ -651,10 +722,10 @@
             pltpu.VMEM((length, channels_dev), BF16),
             pltpu.VMEM((4, length // 4, channels_dev), BF16),
             pltpu.VMEM((tokens, quarter), F32),
-            pltpu.SemaphoreType.DMA((7,)),
+            pltpu.SemaphoreType.DMA((12,)),
             pltpu.SemaphoreType.DMA((22, n_chunks)),
-            pltpu.SemaphoreType.DMA((14,)),
-            pltpu.SemaphoreType.DMA((14,)),
+            pltpu.SemaphoreType.DMA((16,)),
+            pltpu.SemaphoreType.DMA((16,)),
         ],
         compiler_params=pltpu.CompilerParams(
             collective_id=0, has_side_effects=True, vmem_limit_bytes=60 * 1024 * 1024
@@ -669,7 +740,7 @@
         moe_input,
         glu_value,
         glu_gate,
-        out_weight,
+        out_weight.reshape(nyc // 2, 2, channels_dev // nyc, width),
         gate_weight,
         up_weight,
         down_weight,

time: 112 us -> 95 us (0.85)
  Pallas kernels: 108 us -> 92.7 us
  local copies, waits for them, and re-layouts: 3.55 us -> 1.5 us
    pallas_call x1, Pallas kernels: 108 us -> 92.7 us  [on_device(): pl.pallas_call(functools.partial(block_kernel, cfg), out_shape=(pltpu.VME...]
    unnamed x2, local copies, waits for them, and re-layouts: 3.55 us -> 1.5 us
where the time goes in v3:
time: 95 us; the launch traced here: 94.9 us
  Pallas kernels  92.7 us (98%)
  local copies, waits for them, and re-layouts  1.5 us (2%)
    pallas_call x1, Pallas kernels, on_device(): pl.pallas_call(functools.partial(block_kernel, cfg), out_shape=(pltpu.VME...  92.7 us

profile of v3, /device:TPU:1, one launch (start us, length us, event | category | flops | bytes accessed | tf_op | source)
XLA Modules:
  0.0 94.9 jit_solution(8636221936264563866)
XLA Ops:
  0.6 92.7 %block.1 = (bf16[128,2048]{1,0:T(8,128)(2,1)S(1)}, bf16[256,512]{1,0:T(8,128)(2,1)S(1)}) custom-call(f32[1,2048]{1,0:T(1,128)} %bitcast.6, s32[2,256]{1,0:T(2,128)} %bitcast.7, f32[2,256]{1,0:T(2,128)} %bitcast.8, f32[31,256]{1,0:T(8,128)} %taps_hbm.1, f32[1,256]{1,0:T(1,128)} %bitcast.9, bf16[256,2048]{1,0:T(8,128)(2,1)} %moe_hbm.1, ...), custom_call_target="tpu_custom_call" | custom-call | tf_op jit(solution)/shard_map/block/pallas_call | solution.py:683
  93.4 0.8 copy.16
  94.2 0.7 copy.17

commit v4 on v3

--- a/solution.py
+++ b/solution.py
@@ -111,7 +111,7 @@
         )
         return c
 
-    lax.fori_loop(1, n_ep, greet, 0)
+    lax.fori_loop(1, n_ep, greet, 0, unroll=9 if n_ep == 64 else 1)
     for other in (xp, xm, xo):
         pl.semaphore_signal(barrier, inc=1, device_id=(ep, other), device_id_type=MESH)
 
@@ -604,11 +604,6 @@
     run(combine, 1)
     run(give_back, 0)
     run(mixer_project)
-    run(combine, 2)
-    run(combine, 3)
-    run(combine, 0)
-    out[...] = total[...].astype(BF16)
-
     for k in range(n_chunks):
         w0, wn, g0, gn = parts_of(k)
         if wn:
@@ -623,12 +618,10 @@
             region = xin.at[x, pl.ds(g0, gn // 2), :]
             rdma(region, region, FWR_S, FWR_R, k, ep, xp).wait_send()
             rdma(region, region, FWL_S, FWL_R, k, ep, xm).wait_send()
-        back = ans.at[pl.ds(k * rows, rows - less_own(k, bool(whole[own]))), :]
         rdma(s1r.at[k], s1r.at[k], S1R_S, S1R_R, k, ep, xp).wait_send()
         rdma(s1l.at[k], s1l.at[k], S1L_S, S1L_R, k, ep, xm).wait_send()
         rdma(s2r.at[k], s2r.at[k], S2R_S, S2R_R, k, ep, xp).wait_send()
         rdma(s2l.at[k], s2l.at[k], S2L_S, S2L_R, k, ep, xm).wait_send()
-        rdma(back, back, RET_S, RET_R, k, ep, xp).wait_send()
     mcopy(tail, tail, HALO, ep, xp).wait_send()
     for row in (STAT_P, STAT_M, STAT_O):
         mcopy(stat, stat, row, ep, xp).wait_send()
@@ -649,6 +642,13 @@
         mcopy(sent, sent, YFL, y_down, x).wait_send()
     sent = w_out.at[pl.ds(0, 3), :, core]
     mcopy(sent, sent, WC, partner, x).wait_send()
+    run(combine, 2)
+    run(combine, 3)
+    run(combine, 0)
+    out[...] = total[...].astype(BF16)
+    for k in range(n_chunks):
+        back = ans.at[pl.ds(k * rows, rows - less_own(k, bool(whole[own]))), :]
+        rdma(back, back, RET_S, RET_R, k, ep, xp).wait_send()
 
 
 def on_device(

time: 95 us -> 94.7 us (level)
  no operation moved by 1% of the time
where the time goes in v4:
time: 94.7 us; the launch traced here: 94.6 us
  Pallas kernels  92.5 us (98%)
  local copies, waits for them, and re-layouts  1.5 us (2%)
    pallas_call x1, Pallas kernels, on_device(): pl.pallas_call(functools.partial(block_kernel, cfg), out_shape=(pltpu.VME...  92.5 us

profile of v4, /device:TPU:1, one launch (start us, length us, event | category | flops | bytes accessed | tf_op | source)
XLA Modules:
  0.0 94.6 jit_solution(3724523818484935961)
XLA Ops:
  0.6 92.5 %block.1 = (bf16[128,2048]{1,0:T(8,128)(2,1)S(1)}, bf16[256,512]{1,0:T(8,128)(2,1)S(1)}) custom-call(f32[1,2048]{1,0:T(1,128)} %bitcast.6, s32[2,256]{1,0:T(2,128)} %bitcast.7, f32[2,256]{1,0:T(2,128)} %bitcast.8, f32[31,256]{1,0:T(8,128)} %taps_hbm.1, f32[1,256]{1,0:T(1,128)} %bitcast.9, bf16[256,2048]{1,0:T(8,128)(2,1)} %moe_hbm.1, ...), custom_call_target="tpu_custom_call" | custom-call | tf_op jit(solution)/shard_map/block/pallas_call | solution.py:683
  93.1 0.8 copy.16
  93.9 0.7 copy.17
